TPU v7x, 128 devices: a 2x2x16 block of a 8x8x16 slice. The times are simulated.
128 devices in a mesh: grp: 4 (over y, x), ep: 32 (over z, core).
Axes of the slice: x: 2, y: 2, z: 16, core: 2. Of those that a mesh axis runs over, the one named last changes fastest.
The devices are a block of a 8x8x16 slice.
Arguments:
- tokens_in: bfloat16 [256, 4096], P(('grp', 'ep')), parts along dimension 0, may hold values from -6 to 6
- mix_gain: float32 [4096], replicated, may hold values from 0.1 to 1.9
- w_gate_z: bfloat16 [4096, 4096], P(None, 'ep'), may hold values from -0.09375 to 0.09375
- w_value: bfloat16 [4096, 4096], P(None, 'ep'), may hold values from -0.09375 to 0.09375
- w_in_bc: bfloat16 [4096, 1024], P(None, 'ep'), may hold values from -0.09375 to 0.09375
- w_step: bfloat16 [4096, 64], replicated, may hold values from -0.09375 to 0.09375
- step_bias: float32 [64], replicated, may hold values from -4 to 0.5
- decay_log: float32 [64], replicated, may hold values from -1.5 to 2
- skip_gain: float32 [64], replicated, may hold values from 0.3 to 1.7
- conv_x_weight: float32 [4, 4096], replicated, may hold values from -3 to 3
- conv_bc_weight: float32 [4, 1024], replicated, may hold values from -3 to 3
- conv_x_state: bfloat16 [256, 3, 4096], P(('grp', 'ep')), parts along dimension 0, may hold values from -6 to 6
- conv_bc_state: bfloat16 [256, 3, 1024], P(('grp', 'ep')), parts along dimension 0, may hold values from -6 to 6
- ssm_state: float32 [256, 64, 64, 128], P(('grp', 'ep')), parts along dimension 0, may hold values from -3 to 3
- inner_gain: float32 [4096], replicated, may hold values from 0.1 to 1.9
- out_weight: bfloat16 [4096, 4096], P(None, 'ep'), may hold values from -0.09375 to 0.09375
- ffn_gain: float32 [4096], replicated, may hold values from 0.1 to 1.9
- expert_gate: bfloat16 [32, 4096, 512], P('ep'), may hold values from -0.09375 to 0.09375
- expert_up: bfloat16 [32, 4096, 512], P('ep'), may hold values from -0.09375 to 0.09375
- expert_down: bfloat16 [32, 512, 4096], P('ep'), may hold values from -0.25 to 0.25
- routes: int32 [256, 4], P(('grp', 'ep')), parts along dimension 0, may hold values from 0 to 31, all different within a row; in each aligned block of 2 rows (0 to 1, 2 to 3, ...) at most 2 rows name the same one
- route_weight: float32 [256, 4], P(('grp', 'ep')), parts along dimension 0, may hold values from 0.1 to 1
Outputs:
- out_tokens: bfloat16 [256, 4096], P(('grp', 'ep')), parts along dimension 0
- new_state: float32 [256, 64, 64, 128], P(('grp', 'ep')), parts along dimension 0
- new_conv_x: bfloat16 [256, 3, 4096], P(('grp', 'ep')), parts along dimension 0
- new_conv_bc: bfloat16 [256, 3, 1024], P(('grp', 'ep')), parts along dimension 0
There are 4 independent parts, one for each index of `grp`. A program takes and returns all parts, laid end to end along the dimension named above; an argument that names none is the same for every part. Nothing has to cross between parts.
Inputs may be any that keep to these rules, and one draw needn't show every extreme that they name: `routes`: each row names 4 different experts. Among the rows of one device no expert is named more than 2 times, and some device names some expert exactly 2 times.
All inputs are finite; a program needn't handle non-finite values.
Results may differ from a plain program's by a relative error of at most 0.015.
Values may be sent and summed in bfloat16 or wider, within the bound.
A program may use at most 64 MiB of HBM per device.

v0:
```python
import jax
import jax.numpy as jnp
from jax import lax
from jax.sharding import Mesh
from jax.sharding import PartitionSpec as P

HEADS = 64
HEAD_DIM = 64
GROUPS = 4
NSTATE = 128
TOPK = 4
SLOT = 2
EP = ("ep_0", "ep_1")
GRP_EP = ("grp", "ep_0", "ep_1")


def joined_along(tiles, dim):
    lengths = list(tiles.shape[1:])
    lengths[dim] *= tiles.shape[0]
    return jnp.moveaxis(tiles, 0, dim).reshape(lengths)


def copy_for_each(x, axis):
    copies = jnp.broadcast_to(x, (lax.axis_size(axis), *x.shape))
    return lax.all_to_all(copies, axis, split_axis=0, concat_axis=0, tiled=True)


def gathered_copies(x, axis, dim):
    return joined_along(copy_for_each(x, axis), dim)


def gather_in_order(x, axes, sequence):
    tiles = x[None]
    for k in sequence:
        tiles = lax.all_gather(tiles, axes[k], axis=0, tiled=True)
    carried = [lax.axis_size(axes[k]) for k in reversed(sequence)]
    tiles = tiles.reshape(*carried, *x.shape)
    turned = sorted(range(len(sequence)), key=lambda place: sequence[len(sequence) - 1 - place])
    return tiles.transpose(*turned, *range(len(sequence), tiles.ndim)).reshape(-1, *x.shape)


def gather_axes(x, axes, sequence, dim):
    return joined_along(gather_in_order(x, axes, sequence), dim)


def rms_norm(values, gain):
    floats = values.astype(jnp.float32)
    return floats * lax.rsqrt(jnp.mean(floats * floats, axis=-1, keepdims=True) + 1e-06) * gain


def conv_step(window_state, newest, taps):
    window = jnp.concatenate([window_state, newest[:, None, :]], axis=1)
    mixed = jax.nn.silu(jnp.sum(window.astype(jnp.float32) * taps[None, :, :], axis=1))
    return (mixed, window[:, 1:])


def expert_apply(rows, gate_w, up_w, down_w):
    gate_part = jnp.einsum("erd,edf->erf", rows, gate_w, preferred_element_type=jnp.float32)
    up_part = jnp.einsum("erd,edf->erf", rows, up_w, preferred_element_type=jnp.float32)
    act = (jax.nn.silu(gate_part) * up_part).astype(jnp.bfloat16)
    return jnp.einsum("erf,efd->erd", act, down_w, preferred_element_type=jnp.float32).astype(
        jnp.bfloat16
    )


def body(
    tokens_in,
    mix_gain,
    w_gate_z,
    w_value,
    w_in_bc,
    w_step,
    step_bias,
    decay_log,
    skip_gain,
    conv_x_weight,
    conv_bc_weight,
    conv_x_state,
    conv_bc_state,
    ssm_state,
    inner_gain,
    out_weight,
    ffn_gain,
    expert_gate,
    expert_up,
    expert_down,
    routes,
    route_weight,
):
    seq_count = tokens_in.shape[0]
    ep_count = lax.axis_size(EP)
    model_width = tokens_in.shape[1]
    normed = rms_norm(tokens_in, mix_gain).astype(jnp.bfloat16)
    piece = gathered_copies(normed, EP, 0)
    projected = jnp.concatenate(
        [
            jnp.dot(piece, w_gate_z, preferred_element_type=jnp.float32).astype(jnp.bfloat16),
            jnp.dot(piece, w_value, preferred_element_type=jnp.float32).astype(jnp.bfloat16),
            jnp.dot(piece, w_in_bc, preferred_element_type=jnp.float32).astype(jnp.bfloat16),
        ],
        axis=1,
    )
    returned = lax.all_to_all(projected, EP, split_axis=0, concat_axis=1, tiled=True)
    z_width = w_gate_z.shape[1]
    x_width = w_value.shape[1]
    returned = returned.reshape(seq_count, ep_count, -1)
    z_pre = returned[:, :, :z_width].reshape(seq_count, -1)
    x_pre = returned[:, :, z_width : z_width + x_width].reshape(seq_count, -1)
    bc_pre = returned[:, :, z_width + x_width :].reshape(seq_count, -1)
    step_pre = jnp.dot(normed, w_step, preferred_element_type=jnp.float32)
    x_conv, new_conv_x = conv_step(conv_x_state, x_pre, conv_x_weight)
    bc_conv, new_conv_bc = conv_step(conv_bc_state, bc_pre, conv_bc_weight)
    group_cols = GROUPS * NSTATE
    in_map = jnp.repeat(
        bc_conv[:, :group_cols].reshape(seq_count, GROUPS, NSTATE), HEADS // GROUPS, axis=1
    )
    out_map = jnp.repeat(
        bc_conv[:, group_cols:].reshape(seq_count, GROUPS, NSTATE), HEADS // GROUPS, axis=1
    )
    step = jax.nn.softplus(step_pre + step_bias[None, :])
    decay = jnp.exp(-step * jnp.exp(decay_log)[None, :])
    x_heads = x_conv.reshape(seq_count, HEADS, HEAD_DIM)
    new_state = (
        decay[:, :, None, None] * ssm_state
        + (step[:, :, None] * x_heads)[..., None] * in_map[:, :, None, :]
    )
    head_out = jnp.einsum("bhn,bhpn->bhp", out_map, new_state)
    head_out = head_out + skip_gain[None, :, None] * x_heads
    gated = head_out.reshape(seq_count, HEADS * HEAD_DIM) * jax.nn.silu(z_pre.astype(jnp.float32))
    mixed = rms_norm(gated, inner_gain).astype(jnp.bfloat16)
    out_cols = jnp.dot(
        gather_axes(mixed, EP, (0, 1), 0), out_weight, preferred_element_type=jnp.float32
    ).astype(jnp.bfloat16)
    mix_out = lax.all_to_all(out_cols, EP, split_axis=0, concat_axis=1, tiled=True)
    resid = (tokens_in.astype(jnp.float32) + mix_out.astype(jnp.float32)).astype(jnp.bfloat16)
    ffn_in = rms_norm(resid, ffn_gain).astype(jnp.bfloat16)
    local_experts = expert_gate.shape[0]
    n_experts = local_experts * ep_count
    expert_ids = jnp.arange(n_experts, dtype=jnp.int32)
    pair_count = seq_count * TOPK
    flat_routes = routes.reshape(pair_count)
    one_hot = (flat_routes[:, None] == expert_ids[None, :]).astype(jnp.int32)
    earlier = jnp.cumsum(one_hot, axis=0) - one_hot
    slot_index = jnp.sum(earlier * one_hot, axis=1)
    target = flat_routes * SLOT + slot_index
    slot_ids = jnp.arange(n_experts * SLOT, dtype=jnp.int32)
    placing = (slot_ids[:, None] == target[None, :]).astype(jnp.bfloat16)
    pair_rows = jnp.repeat(ffn_in, TOPK, axis=0)
    outgoing = jnp.dot(placing, pair_rows, preferred_element_type=jnp.float32).astype(jnp.bfloat16)
    outgoing = outgoing.reshape(n_experts, 1, SLOT, model_width)
    received = lax.all_to_all(outgoing, EP, split_axis=0, concat_axis=1, tiled=True)
    slot_count = received.shape[2]
    rows = received.reshape(local_experts, ep_count * slot_count, model_width)
    expert_rows = expert_apply(rows, expert_gate, expert_up, expert_down)
    expert_rows = expert_rows.reshape(local_experts, ep_count, slot_count, model_width)
    came_back = lax.all_to_all(expert_rows, EP, split_axis=1, concat_axis=0, tiled=True)
    came_back = came_back.reshape(n_experts * SLOT, model_width)
    pair_out = jnp.dot(jnp.transpose(placing), came_back, preferred_element_type=jnp.float32)
    weighted = pair_out * route_weight.reshape(pair_count)[:, None]
    summed = jnp.sum(weighted.reshape(seq_count, TOPK, model_width), axis=1)
    out_tokens = (resid.astype(jnp.float32) + summed).astype(jnp.bfloat16)
    return (out_tokens, new_state, new_conv_x, new_conv_bc)


def solution(mesh):
    torus = Mesh(mesh.devices.reshape(mesh.shape["grp"], 16, 2), ("grp", "ep_0", "ep_1"))
    placed = (
        P(GRP_EP, None),
        P(),
        P(None, EP),
        P(None, EP),
        P(None, EP),
        P(),
        P(),
        P(),
        P(),
        P(),
        P(),
        P(GRP_EP, None, None),
        P(GRP_EP, None, None),
        P(GRP_EP, None, None, None),
        P(),
        P(None, EP),
        P(),
        P(EP, None, None),
        P(EP, None, None),
        P(EP, None, None),
        P(GRP_EP, None),
        P(GRP_EP, None),
    )
    return jax.shard_map(
        body,
        mesh=torus,
        in_specs=placed,
        out_specs=(
            P(GRP_EP, None),
            P(GRP_EP, None, None, None),
            P(GRP_EP, None, None),
            P(GRP_EP, None, None),
        ),
        check_vma=False,
    )
```

profile of v0, /device:TPU:69, one launch (start us, length us, event | category | flops | bytes accessed | tf_op | source)
XLA Modules:
  0.0 220.4 jit_solution(9496159974318079421)
XLA Ops:
  0.7 1.0 fusion.21
  1.7 0.8 fusion.23
  2.5 1.3 broadcast_in_dim.8
  3.8 18.5 %all-to-all-start = ((bf16[32,2,4096]{2,1,0:T(2,128)(2,1)}), bf16[32,2,4096]{2,1,0:T(2,128)(2,1)S(1)}, u32[]{:S(2)}, u32[]{:S(2)}) async-start(bf16[32,2,4096]{2,1,0:T(2,128)(2,1)} %broadcast_in_dim.8), calls=%async_computation | async-start | bytes 1048576 | tf_op jit(solution)/shard_map/all_to_all | solution.py:25
  22.3 0.7 exp.43
  23.0 0.8 reshape.248
  23.8 1.3 multiply_exponential_fusion
  25.2 30.5 %all-to-all-done = bf16[32,2,4096]{2,1,0:T(2,128)(2,1)S(1)} async-done(((bf16[32,2,4096]{2,1,0:T(2,128)(2,1)}), bf16[32,2,4096]{2,1,0:T(2,128)(2,1)S(1)}, u32[]{:S(2)}, u32[]{:S(2)}) %all-to-all-start) | async-done | bytes 524320 | tf_op jit(solution)/shard_map/all_to_all | solution.py:25
  55.6 0.2 reshape.242
  55.8 1.2 convolution_convert_fusion.5
  57.1 0.1 copy.61
  57.2 0.3 convolution_convert_fusion.3
  57.5 0.3 convolution_convert_fusion.4
  57.8 0.6 all_to_all.19
  58.5 4.2 %all-to-all-start.1 = ((bf16[32,2,288]{2,1,0:T(2,128)(2,1)}), bf16[32,2,288]{2,1,0:T(2,128)(2,1)S(1)}, u32[]{:S(2)}, u32[]{:S(2)}) async-start(bf16[32,2,288]{2,1,0:T(2,128)(2,1)} %all_to_all.19), calls=%async_computation.1 | async-start | bytes 98304 | tf_op jit(solution)/shard_map/all_to_all | solution.py:103
  62.8 0.2 select_reduce_fusion
  63.0 12.3 %all-to-all-done.1 = bf16[32,2,288]{2,1,0:T(2,128)(2,1)S(1)} async-done(((bf16[32,2,288]{2,1,0:T(2,128)(2,1)}), bf16[32,2,288]{2,1,0:T(2,128)(2,1)S(1)}, u32[]{:S(2)}, u32[]{:S(2)}) %all-to-all-start.1) | async-done | bytes 36896 | tf_op jit(solution)/shard_map/all_to_all | solution.py:103
  75.4 0.1 multiply_reduce_fusion
  75.5 0.1 reduce_sum.68
  75.6 0.1 broadcast_in_dim_reshape.4
  76.0 3.8 %multiply_add_fusion = f32[2,64,64,128]{3,2,1,0:T(8,128)S(1)} fusion(f32[2,64,64,128]{3,2,1,0:T(8,128)} %param.35, f32[2,64,128]{2,1,0:T(8,128)S(1)} %bitcast.76, f32[2,64,64]{2,1,0:T(8,128)S(1)} %broadcast_multiply_fusion, f32[2,64]{1,0:T(2,128)S(1)} %get-tuple-element.10), kind=kLoop, calls=%fused_computation.8 | loop fusion | flops 3145728 | bytes 8487424 | tf_op jit(solution)/shard_map/add | solution.py:124
  79.8 2.0 copy-done.1
  81.8 1.2 fusion.36
  83.0 0.2 multiply_reduce_fusion.1
  83.2 0.1 reshape.246
  83.4 21.5 %all_gather.6 = bf16[16,2,4096]{2,1,0:T(2,128)(2,1)S(1)} all-gather(bf16[1,2,4096]{2,1,0:T(2,128)(2,1)S(1)} %multiply_convert_fusion), channel_id=1, replica_groups=mesh['grp'=4,'ep_0'=16,'ep_1'=2] {'ep_0'}, dimensions={0}, use_global_device_ids=true | all-gather | bytes 278528 | tf_op jit(solution)/shard_map/all_gather | solution.py:35
  104.9 0.1 copy.64
  105.1 9.8 %all_gather.7 = bf16[32,2,4096]{2,0,1:T(8,128)(2,1)S(1)} all-gather(bf16[16,2,4096]{2,0,1:T(8,128)(2,1)S(1)} %copy.64), channel_id=1, replica_groups=mesh['grp'=4,'ep_0'=16,'ep_1'=2] {'ep_1'}, dimensions={0}, use_global_device_ids=true | all-gather | bytes 786432 | tf_op jit(solution)/shard_map/all_gather | solution.py:35
  114.8 0.5 copy.65
  115.4 0.2 reshape_reshape.3
  115.6 0.9 convolution_convert_fusion.2
  116.5 5.6 %all-to-all-start.2 = ((bf16[32,2,128]{2,1,0:T(2,128)(2,1)}), bf16[32,2,128]{2,1,0:T(2,128)(2,1)S(1)}, u32[]{:S(2)}, u32[]{:S(2)}) async-start(bf16[32,2,128]{2,1,0:T(2,128)(2,1)} %bitcast.11), calls=%async_computation.2 | async-start | bytes 32768 | tf_op jit(solution)/shard_map/all_to_all | solution.py:134
  122.1 11.5 %all-to-all-done.2 = bf16[32,2,128]{2,1,0:T(2,128)(2,1)S(1)} async-done(((bf16[32,2,128]{2,1,0:T(2,128)(2,1)}), bf16[32,2,128]{2,1,0:T(2,128)(2,1)S(1)}, u32[]{:S(2)}, u32[]{:S(2)}) %all-to-all-start.2) | async-done | bytes 16416 | tf_op jit(solution)/shard_map/all_to_all | solution.py:134
  133.6 0.1 fusion.25
  133.9 0.3 convolution_convert_fusion.1
  134.2 0.3 reshape.250
  134.5 37.2 %all_to_all.52 = bf16[32,1,2,4096]{3,2,1,0:T(2,128)(2,1)S(1)} all-to-all(bf16[32,1,2,4096]{3,2,1,0:T(2,128)(2,1)S(1)} %bitcast.72), channel_id=1, replica_groups=mesh['grp'=4,'ep_0'=16,'ep_1'=2] {'ep_0','ep_1'}, dimensions={0} | all-to-all | bytes 1048576 | tf_op jit(solution)/shard_map/all_to_all | solution.py:151
  171.8 0.2 reshape.251
  172.0 3.0 %fusion.3 = f32[64,512]{1,0:T(8,128)S(1)} fusion(bf16[64,4096]{1,0:T(8,128)(2,1)S(1)} %reshape.251, bf16[1,4096,512]{2,1,0:T(8,128)(2,1)} %param.39), kind=kOutput, calls=%fused_computation.6 | convolution fusion | flops 268435456 | bytes 4849664 | tf_op jit(solution)/shard_map/erd,edf->erf/dot_general | solution.py:58
  175.0 5.1 %convolution_convert_fusion = bf16[64,4096]{1,0:T(8,128)(2,1)S(1)} fusion(bf16[1,512,4096]{2,1,0:T(8,128)(2,1)} %param.41, bf16[64,4096]{1,0:T(8,128)(2,1)S(1)} %reshape.251, bf16[1,4096,512]{2,1,0:T(8,128)(2,1)} %param.40, f32[64,512]{1,0:T(8,128)S(1)} %fusion.3), kind=kOutput, calls=%fused_computation | convolution fusion | flops 537329664 | bytes 9568256 | tf_op jit(solution)/shard_map/erf,efd->erd/dot_general | solution.py:61
  180.1 1.1 reshape.255
  181.2 4.6 %all-to-all-start.4 = ((bf16[1,32,2,4096]{3,2,0,1:T(2,128)(2,1)}), bf16[1,32,2,4096]{3,2,0,1:T(2,128)(2,1)S(1)}, u32[]{:S(2)}, u32[]{:S(2)}) async-start(bf16[1,32,2,4096]{3,2,0,1:T(2,128)(2,1)} %bitcast.18), calls=%async_computation.4 | async-start | bytes 1048576 | tf_op jit(solution)/shard_map/all_to_all | solution.py:156
  185.9 0.6 slice.35
  186.5 0.7 fusion.19
  187.2 32.0 %all-to-all-done.4 = bf16[1,32,2,4096]{3,2,0,1:T(2,128)(2,1)S(1)} async-done(((bf16[1,32,2,4096]{3,2,0,1:T(2,128)(2,1)}), bf16[1,32,2,4096]{3,2,0,1:T(2,128)(2,1)S(1)}, u32[]{:S(2)}, u32[]{:S(2)}) %all-to-all-start.4) | async-done | bytes 524320 | tf_op jit(solution)/shard_map/all_to_all | solution.py:156
  219.2 0.2 reshape.256
  219.4 0.2 convolution_multiply_fusion
  219.8 0.6 fusion.28
  (54 shorter events, 1.0 us)
Async XLA Ops:
  0.6 56.5 %copy-start = (bf16[4096,128]{1,0:T(8,128)(2,1)S(1)}, bf16[4096,128]{1,0:T(8,128)(2,1)}, u32[]{:S(2)}) copy-start(bf16[4096,128]{1,0:T(8,128)(2,1)} %param.25) | copy-start | bytes 3145732
  0.6 56.8 %copy-start.2 = (bf16[4096,128]{1,0:T(8,128)(2,1)S(1)}, bf16[4096,128]{1,0:T(8,128)(2,1)}, u32[]{:S(2)}) copy-start(bf16[4096,128]{1,0:T(8,128)(2,1)} %param.24) | copy-start | bytes 3145732
  0.7 62.1 %copy-start.10 = (bf16[2,3,1024]{2,0,1:T(2,128)(2,1)S(1)}, bf16[2,3,1024]{2,0,1:T(2,128)(2,1)}, u32[]{:S(2)}) copy-start(bf16[2,3,1024]{2,0,1:T(2,128)(2,1)} %param.34) | copy-start | bytes 36868
  0.7 74.7 %copy-start.6 = (f32[4,4096]{1,0:T(4,128)S(1)}, f32[4,4096]{1,0:T(4,128)}, u32[]{:S(2)}) copy-start(f32[4,4096]{1,0:T(4,128)} %param.31) | copy-start | bytes 196612
  0.7 74.7 %copy-start.5 = (bf16[2,3,4096]{2,0,1:T(2,128)(2,1)S(1)}, bf16[2,3,4096]{2,0,1:T(2,128)(2,1)}, u32[]{:S(2)}) copy-start(bf16[2,3,4096]{2,0,1:T(2,128)(2,1)} %param.33) | copy-start | bytes 147460
  0.7 75.0 %copy-start.8 = (f32[4,1024]{1,0:T(4,128)S(1)}, f32[4,1024]{1,0:T(4,128)}, u32[]{:S(2)}) copy-start(f32[4,1024]{1,0:T(4,128)} %param.32) | copy-start | bytes 49156
  3.8 51.8 %all-to-all-start = ((bf16[32,2,4096]{2,1,0:T(2,128)(2,1)}), bf16[32,2,4096]{2,1,0:T(2,128)(2,1)S(1)}, u32[]{:S(2)}, u32[]{:S(2)}) async-start(bf16[32,2,4096]{2,1,0:T(2,128)(2,1)} %broadcast_in_dim.8), calls=%async_computation | async-start | bytes 1048576 | tf_op jit(solution)/shard_map/all_to_all | solution.py:25
  58.5 16.8 %all-to-all-start.1 = ((bf16[32,2,288]{2,1,0:T(2,128)(2,1)}), bf16[32,2,288]{2,1,0:T(2,128)(2,1)S(1)}, u32[]{:S(2)}, u32[]{:S(2)}) async-start(bf16[32,2,288]{2,1,0:T(2,128)(2,1)} %all_to_all.19), calls=%async_computation.1 | async-start | bytes 98304 | tf_op jit(solution)/shard_map/all_to_all | solution.py:103
  79.8 2.0 copy-start.1
  79.8 3.2 %copy-start.11 = (f32[64]{0:T(128)S(1)}, f32[64]{0:T(128)}, u32[]{:S(2)}) copy-start(f32[64]{0:T(128)} %param.30) | copy-start | bytes 772
  79.8 3.5 %copy-start.7 = (f32[4096]{0:T(1024)S(1)}, f32[4096]{0:T(1024)}, u32[]{:S(2)}) copy-start(f32[4096]{0:T(1024)} %param.36) | copy-start | bytes 49156
  81.8 33.8 %copy-start.3 = (bf16[4096,128]{1,0:T(8,128)(2,1)S(1)}, bf16[4096,128]{1,0:T(8,128)(2,1)}, u32[]{:S(2)}) copy-start(bf16[4096,128]{1,0:T(8,128)(2,1)} %param.37) | copy-start | bytes 3145732
  81.8 51.8 %copy-start.4 = (bf16[2,4096]{1,0:T(2,128)(2,1)S(1)}, bf16[2,4096]{1,0:T(2,128)(2,1)}, u32[]{:S(2)}) copy-start(bf16[2,4096]{1,0:T(2,128)(2,1)} %param.22) | copy-start | bytes 49156
  81.8 51.9 %copy-start.9 = (f32[4096]{0:T(1024)S(1)}, f32[4096]{0:T(1024)}, u32[]{:S(2)}) copy-start(f32[4096]{0:T(1024)} %param.38) | copy-start | bytes 49156
  116.5 17.1 %all-to-all-start.2 = ((bf16[32,2,128]{2,1,0:T(2,128)(2,1)}), bf16[32,2,128]{2,1,0:T(2,128)(2,1)S(1)}, u32[]{:S(2)}, u32[]{:S(2)}) async-start(bf16[32,2,128]{2,1,0:T(2,128)(2,1)} %bitcast.11), calls=%async_computation.2 | async-start | bytes 32768 | tf_op jit(solution)/shard_map/all_to_all | solution.py:134
  175.0 10.8 %copy-start.12 = (f32[2,4]{1,0:T(2,128)S(1)}, f32[2,4]{1,0:T(2,128)}, u32[]{:S(2)}) copy-start(f32[2,4]{1,0:T(2,128)} %param.43) | copy-start | bytes 100
  181.2 38.0 %all-to-all-start.4 = ((bf16[1,32,2,4096]{3,2,0,1:T(2,128)(2,1)}), bf16[1,32,2,4096]{3,2,0,1:T(2,128)(2,1)S(1)}, u32[]{:S(2)}, u32[]{:S(2)}) async-start(bf16[1,32,2,4096]{3,2,0,1:T(2,128)(2,1)} %bitcast.18), calls=%async_computation.4 | async-start | bytes 1048576 | tf_op jit(solution)/shard_map/all_to_all | solution.py:156
where the time goes:
time: 221 us; the launch traced here: 220 us
  waiting for transfers between devices  86.3 us (39%)
  blocking collectives  68.5 us (31%)
  starting transfers between devices  32.9 us (15%)
  matrix products  13.9 us (6%)
  local copies, waits for them, and re-layouts  9.65 us (4%)
  other arithmetic  8.15 us (4%)
    all_to_all x1, blocking collectives, body(): lax.all_to_all(outgoing, EP, split_axis=0, concat_axis=1, tiled=True)  37.2 us
    all_to_all x1, waiting for transfers between devices, body(): lax.all_to_all(expert_rows, EP, split_axis=1, concat_axis=0, tiled=True)  32 us
    all_gather x2, blocking collectives, gather_in_order(): tiles = lax.all_gather(tiles, axes[k], axis=0, tiled=True)  31.3 us
    all_to_all x1, waiting for transfers between devices, copy_for_each(): return lax.all_to_all(copies, axis, split_axis=0, concat_axis=0, tiled=True)  30.5 us
    all_to_all x1, starting transfers between devices, copy_for_each(): return lax.all_to_all(copies, axis, split_axis=0, concat_axis=0, tiled=True)  18.5 us
    all_to_all x1, waiting for transfers between devices, body(): lax.all_to_all(projected, EP, split_axis=0, concat_axis=1, tiled=True)  12.3 us
    all_to_all x1, waiting for transfers between devices, body(): lax.all_to_all(out_cols, EP, split_axis=0, concat_axis=1, tiled=True)  11.5 us
    all_to_all x1, starting transfers between devices, body(): lax.all_to_all(out_cols, EP, split_axis=0, concat_axis=1, tiled=True)  5.58 us
  transfers between devices with their start and end apart: 4, of which 4 were waited for; matrix products, arithmetic and copies ran while one was open for 2% of the time, Pallas kernels for 0%

commit v1 on v0

v1 whole, which is shorter than its diff:
```python
import functools

import jax
import jax.numpy as jnp
from jax import lax
from jax.experimental import pallas as pl
from jax.experimental.pallas import tpu as pltpu
from jax.sharding import PartitionSpec as P

HEADS = 64
HEAD_DIM = 64
GROUPS = 4
NSTATE = 128
TOPK = 4
GRP_EP = ("grp", "ep")
MESH = pl.DeviceIdType.MESH
F32 = jnp.float32
BF16 = jnp.bfloat16
LANES = 128
PITCH = 40

OWN = (6, -6, 3, -3, 1, -1)
RELAYS = (3, -3, 6, -6)


class Comm:
    def __init__(self, ep):
        self.ep = ep
        self.nz = ep // 2
        self.me = lax.axis_index("ep")
        self.core = lax.rem(self.me, 2)
        self.z = lax.div(self.me, 2)

    def at(self, offset, core):
        return lax.rem(self.z + offset + self.nz, self.nz) * 2 + core

    def partner(self):
        return self.z * 2 + (1 - self.core)

    def barrier(self):
        sem = pltpu.get_barrier_semaphore()

        def greet(i, carry):
            pl.semaphore_signal(
                sem, inc=1, device_id={"ep": lax.rem(self.me + i, self.ep)}, device_id_type=MESH
            )
            return carry

        lax.fori_loop(1, self.ep, greet, 0)
        return lambda: pl.semaphore_wait(sem, self.ep - 1)

    def copy(self, src, dst, send, recv, to):
        return pltpu.make_async_remote_copy(
            src_ref=src, dst_ref=dst, send_sem=send, recv_sem=recv, device_id={"ep": to}, device_id_type=MESH
        )

    def gather(self, buf, send, recv, landed):
        core, me = self.core, self.me

        def pass_on(block, to):
            self.copy(buf.at[block], buf.at[block], send, recv.at[block], to).start()

        def arrive(block):
            self.copy(buf.at[block], buf.at[block], send, recv.at[block], me).wait_recv()

        for d in OWN:
            pass_on(me, self.at(d, core))
        pass_on(me, self.partner())
        landed(me)
        extra = 2 - 4 * core
        for d in RELAYS:
            block = self.at(-d, core)
            arrive(block)
            pass_on(block, self.at(1, core))
            pass_on(block, self.at(-1, core))
            if d == 6:

                @pl.when(core == 0)
                def _(block=block):
                    pass_on(block, self.at(2, core))

            if d == -6:

                @pl.when(core == 1)
                def _(block=block):
                    pass_on(block, self.at(-2, core))

            pass_on(block, self.partner())
            landed(block)
        del extra
        for d in (1, -1, 2, -2, 4, -4, 5, -5, 7, -7, 8):
            block = self.at(-d, core)
            arrive(block)
            pass_on(block, self.partner())
            landed(block)

        def other(i, carry):
            block = self.at(i, 1 - core)
            arrive(block)
            landed(block)
            return carry

        lax.fori_loop(0, self.nz, other, 0)
        n = self.nz - 1 + self.nz
        whole = buf.at[pl.ds(0, n)]
        self.copy(whole, whole, send, recv.at[0], me).wait_send()

    def exchange(self, out, back, send, recv):
        me, ep, nz = self.me, self.ep, self.nz

        def one(to):
            self.copy(out.at[to], back.at[me], send, recv.at[me], to).start()

        def far_first(k, carry):
            offset = (nz // 2 - lax.div(k + 1, 2)) * (1 - 2 * lax.rem(k, 2))
            one(self.at(offset, 0))
            one(self.at(offset, 1))
            return carry

        lax.fori_loop(0, nz - 1, far_first, 0)
        one(self.partner())
        back[me] = out[me]

    def exchanged(self, out, back, send, recv, landed):
        me, ep = self.me, self.ep
        landed(me)

        def one(i, carry):
            frm = lax.rem(me + i, ep)
            self.copy(back.at[frm], back.at[frm], send, recv.at[frm], me).wait_recv()
            landed(frm)
            return carry

        lax.fori_loop(1, ep, one, 0)
        whole = out.at[pl.ds(0, ep - 1)]
        self.copy(whole, whole, send, recv.at[0], me).wait_send()


def tall(x, n):
    return x.reshape(n, x.shape[0] // n, x.shape[1])


def project_kernel(
    ep, tok_hbm, gain, wz_hbm, wx_hbm, wbc_hbm, wst_hbm, routes, weights,
    r_out, xraw_out, own_out,
    buf, stage, lhs, wz, wx, wbc, wst, flat, out, back,
    load, wload, gsend, grecv, xsend, xrecv,
):
    comm = Comm(ep)
    me = comm.me
    ready = comm.barrier()
    own = pltpu.make_async_copy(tok_hbm, buf.at[me], load)
    own.start()
    pulls = [
        pltpu.make_async_copy(a, b, wload.at[i])
        for i, (a, b) in enumerate(((wz_hbm, wz), (wx_hbm, wx), (wbc_hbm, wbc), (wst_hbm, wst)))
    ]
    for p in pulls:
        p.start()
    own.wait()
    ready()

    def landed(block):
        both = buf[block].astype(F32)
        for r in range(2):
            stage[pl.ds(pl.multiple_of((block * 2 + r) * PITCH, 8), 32), :] = both[r]

    comm.gather(buf, gsend, grecv, landed)
    square = jnp.zeros((64, LANES), F32)
    for j in range(32):
        x = stage[pl.ds(j, 64, stride=PITCH), :]
        square = square + x * x
        xraw_out[:, j * LANES : (j + 1) * LANES] = x.astype(BF16)
        lhs[:, j * LANES : (j + 1) * LANES] = (x * gain[j : j + 1, :]).astype(BF16)
    scale = lax.rsqrt(jnp.sum(square, axis=1, keepdims=True) / 4096.0 + 1e-6)
    for p in pulls:
        p.wait()
    left = lhs[...]
    z = jnp.dot(left, wz[...], preferred_element_type=F32) * scale
    x = jnp.dot(left, wx[...], preferred_element_type=F32) * scale
    bc = jnp.dot(left, wbc[...], preferred_element_type=F32) * scale
    st = jnp.dot(left, wst[...], preferred_element_type=F32) * scale
    lane = lax.broadcasted_iota(jnp.int32, (1, LANES), 1)
    spread = jnp.concatenate([bc, bc, bc, bc], axis=1)
    spread = jnp.where(lax.div(lane, 32) == lax.rem(me, 4), spread, 0.0)
    flat[pl.ds(0, 64, stride=4), :] = z
    flat[pl.ds(1, 64, stride=4), :] = x
    flat[pl.ds(2, 64, stride=4), :] = spread
    dense = jnp.zeros((1, LANES), F32)
    for r in range(2):
        for k in range(TOPK):
            dense = dense + jnp.where(lane == routes[r, k] + 32 * r, weights[r, k], 0.0)
    high = dense.astype(BF16).astype(F32)
    flat[pl.ds(3, 32, stride=8), :] = jnp.broadcast_to(high, (32, LANES))
    flat[pl.ds(7, 32, stride=8), :] = jnp.broadcast_to(dense - high, (32, LANES))
    out[...] = tall(flat[...], 32).astype(BF16)
    comm.exchange(out, back, xsend, xrecv)
    own_out[...] = st
    comm.exchanged(out, back, xsend, xrecv, lambda frm: None)
    r_out[...] = back[...]


def mix_kernel(
    ep, mix_hbm, xraw, r_in, gain, wo_hbm, wg_hbm, wu_hbm, wd_hbm,
    out_ref,
    buf, buf3, stage, lhs, wo, wg, wu, wd, act, flat, wide, half_out, half_in, mine, send_rows, got_rows, total,
    load, wload, gsend, grecv, gsend3, grecv3, hsend, hrecv, xsend, xrecv,
):
    comm = Comm(ep)
    me, core = comm.me, comm.core
    ready = comm.barrier()
    own = pltpu.make_async_copy(mix_hbm, buf.at[me], load)
    own.start()
    pulls = [
        pltpu.make_async_copy(a, b, wload.at[i])
        for i, (a, b) in enumerate(((wo_hbm, wo), (wg_hbm.at[0], wg), (wu_hbm.at[0], wu), (wd_hbm.at[0], wd)))
    ]
    for p in pulls:
        p.start()
    flat[...] = r_in[...].astype(F32).reshape(256, LANES)
    lane = lax.broadcasted_iota(jnp.int32, (32, LANES), 1)
    dense = flat[pl.ds(3, 32, stride=8), :] + flat[pl.ds(7, 32, stride=8), :]
    for r in range(2):
        picked = jnp.sum(jnp.where(lane == me + 32 * r, dense, 0.0), axis=1, keepdims=True)
        wide[pl.ds(r, 32, stride=2), :] = jnp.broadcast_to(picked, (32, LANES))
    own.wait()
    ready()

    def landed(block):
        both = buf[block].astype(F32)
        for r in range(2):
            stage[pl.ds(pl.multiple_of((block * 2 + r) * PITCH, 8), 32), :] = both[r]

    comm.gather(buf, gsend, grecv, landed)
    for j in range(32):
        lhs[:, j * LANES : (j + 1) * LANES] = stage[pl.ds(j, 64, stride=PITCH), :].astype(BF16)
    pulls[0].wait()
    buf3[me] = jnp.dot(lhs[...], wo[...], preferred_element_type=F32).astype(BF16)
    comm.gather(buf3, gsend3, grecv3, lambda block: None)
    square = jnp.zeros((64, LANES), F32)
    for j in range(32):
        cols = slice(j * LANES, (j + 1) * LANES)
        resid = (xraw[:, cols].astype(F32) + buf3[j].astype(F32)).astype(BF16).astype(F32)
        square = square + resid * resid
        stage[pl.ds(j, 64, stride=PITCH), :] = resid
        lhs[:, cols] = (resid * gain[j : j + 1, :]).astype(BF16)
    scale = lax.rsqrt(jnp.sum(square, axis=1, keepdims=True) / 4096.0 + 1e-6)
    pulls[1].wait()
    pulls[2].wait()
    left = lhs[...]
    g = jnp.dot(left, wg[...], preferred_element_type=F32) * scale
    u = jnp.dot(left, wu[...], preferred_element_type=F32) * scale
    act[...] = (jax.nn.silu(g) * u).astype(BF16)
    pulls[3].wait()
    weight = wide[...]

    def rows(half, k):
        cols = pl.ds(pl.multiple_of(half * 2048 + k * 512, 512), 512)
        y = jnp.dot(act[...], wd[:, cols], preferred_element_type=F32).astype(BF16).astype(F32)
        return y * jnp.concatenate([weight] * 4, axis=1)

    for k in range(4):
        half_out[:, k * 512 : (k + 1) * 512] = rows(1 - core, k).astype(BF16)
    swap = comm.copy(half_out, half_in, hsend, hrecv, comm.partner())
    swap.start()
    for k in range(4):
        mine[:, k * 512 : (k + 1) * 512] = rows(core, k)
    swap.wait()
    for j in range(16):
        cols = slice(j * LANES, (j + 1) * LANES)
        total[pl.ds(j, 64, stride=24), :] = mine[:, cols] + half_in[:, cols].astype(F32)

    def pack(t, carry):
        for r in range(2):
            send_rows[t, r] = total[pl.ds(pl.multiple_of((t * 2 + r) * 24, 8), 16), :].astype(BF16)
        return carry

    lax.fori_loop(0, ep, pack, 0)
    comm.exchange(send_rows, got_rows, xsend, xrecv)
    for r in range(2):
        total[pl.ds(r * 32, 32), :] = stage[pl.ds(pl.multiple_of((me * 2 + r) * PITCH, 8), 32), :]

    def arrived(frm):
        h = lax.rem(frm, 2)
        for r in range(2):
            at = pl.ds(pl.multiple_of(r * 32 + h * 16, 8), 16)
            total[at, :] = total[at, :] + got_rows[frm, r].astype(F32)

    comm.exchanged(send_rows, got_rows, xsend, xrecv, arrived)
    out_ref[...] = total[pl.ds(0, 64), :].astype(BF16)


def vmem():
    return pl.BlockSpec(memory_space=pltpu.VMEM)


def hbm():
    return pl.BlockSpec(memory_space=pl.ANY)


def smem():
    return pl.BlockSpec(memory_space=pltpu.SMEM)


def project(ep, tok, gain, wz, wx, wbc, wst, routes, weights):
    dma = pltpu.SemaphoreType.DMA
    return pl.pallas_call(
        functools.partial(project_kernel, ep),
        out_shape=(
            jax.ShapeDtypeStruct((ep, 8, LANES), BF16),
            jax.ShapeDtypeStruct((64, 4096), BF16),
            jax.ShapeDtypeStruct((64, 64), F32),
        ),
        in_specs=[hbm(), vmem(), hbm(), hbm(), hbm(), hbm(), smem(), smem()],
        out_specs=(vmem(), vmem(), vmem()),
        scratch_shapes=[
            pltpu.VMEM((ep, 2, 32, LANES), BF16),
            pltpu.VMEM((64 * PITCH, LANES), F32),
            pltpu.VMEM((64, 4096), BF16),
            pltpu.VMEM(wz.shape, BF16),
            pltpu.VMEM(wx.shape, BF16),
            pltpu.VMEM(wbc.shape, BF16),
            pltpu.VMEM(wst.shape, BF16),
            pltpu.VMEM((256, LANES), F32),
            pltpu.VMEM((ep, 8, LANES), BF16),
            pltpu.VMEM((ep, 8, LANES), BF16),
            dma, dma((4,)), dma, dma((ep,)), dma, dma((ep,)),
        ],
        compiler_params=pltpu.CompilerParams(collective_id=0, has_side_effects=True),
        name="project",
    )(tok, gain, wz, wx, wbc, wst, routes, weights)


def mix(ep, mixed, xraw, r, gain, wo, wg, wu, wd):
    dma = pltpu.SemaphoreType.DMA
    return pl.pallas_call(
        functools.partial(mix_kernel, ep),
        out_shape=jax.ShapeDtypeStruct((64, LANES), BF16),
        in_specs=[hbm(), vmem(), vmem(), vmem(), hbm(), hbm(), hbm(), hbm()],
        out_specs=vmem(),
        scratch_shapes=[
            pltpu.VMEM((ep, 2, 32, LANES), BF16),
            pltpu.VMEM((ep, 64, LANES), BF16),
            pltpu.VMEM((64 * PITCH, LANES), F32),
            pltpu.VMEM((64, 4096), BF16),
            pltpu.VMEM(wo.shape, BF16),
            pltpu.VMEM(wg.shape[1:], BF16),
            pltpu.VMEM(wu.shape[1:], BF16),
            pltpu.VMEM(wd.shape[1:], BF16),
            pltpu.VMEM((64, 512), BF16),
            pltpu.VMEM((256, LANES), F32),
            pltpu.VMEM((64, LANES), F32),
            pltpu.VMEM((64, 2048), BF16),
            pltpu.VMEM((64, 2048), BF16),
            pltpu.VMEM((64, 2048), F32),
            pltpu.VMEM((ep, 2, 16, LANES), BF16),
            pltpu.VMEM((ep, 2, 16, LANES), BF16),
            pltpu.VMEM((64 * 24, LANES), F32),
            dma, dma((4,)), dma, dma((ep,)), dma, dma((ep,)), dma, dma, dma, dma((ep,)),
        ],
        compiler_params=pltpu.CompilerParams(collective_id=1, has_side_effects=True),
        name="mix",
    )(mixed, xraw, r, gain, wo, wg, wu, wd)


def rms_norm(values, gain):
    floats = values.astype(jnp.float32)
    return floats * lax.rsqrt(jnp.mean(floats * floats, axis=-1, keepdims=True) + 1e-06) * gain


def conv_step(window_state, newest, taps):
    window = jnp.concatenate([window_state, newest[:, None, :]], axis=1)
    mixed = jax.nn.silu(jnp.sum(window.astype(jnp.float32) * taps[None, :, :], axis=1))
    return (mixed, window[:, 1:])


def body(
    ep, tokens_in, mix_gain, w_gate_z, w_value, w_in_bc, w_step, step_bias, decay_log, skip_gain, conv_x_weight,
    conv_bc_weight, conv_x_state, conv_bc_state, ssm_state, inner_gain, out_weight, ffn_gain, expert_gate,
    expert_up, expert_down, routes, route_weight,
):
    seqs, width = tokens_in.shape
    r, xraw, st = project(
        ep, tokens_in.reshape(2, 32, LANES), mix_gain.reshape(32, LANES), w_gate_z, w_value, w_in_bc, w_step,
        routes, route_weight,
    )
    tiles = r.reshape(ep, 2, 4, LANES)
    z_pre = tiles[:, :, 0].transpose(1, 0, 2).reshape(seqs, -1)
    x_pre = tiles[:, :, 1].transpose(1, 0, 2).reshape(seqs, -1)
    bc_pre = tiles[:, :, 2].astype(F32).reshape(8, 4, 2, LANES).sum(1).astype(BF16)
    bc_pre = bc_pre.transpose(1, 0, 2).reshape(seqs, -1)
    me = lax.axis_index("ep")
    step_pre = lax.dynamic_slice_in_dim(st, me * 2, 2, 0)
    x_conv, new_conv_x = conv_step(conv_x_state, x_pre, conv_x_weight)
    bc_conv, new_conv_bc = conv_step(conv_bc_state, bc_pre, conv_bc_weight)
    group_cols = GROUPS * NSTATE
    in_map = jnp.repeat(bc_conv[:, :group_cols].reshape(seqs, GROUPS, NSTATE), HEADS // GROUPS, axis=1)
    out_map = jnp.repeat(bc_conv[:, group_cols:].reshape(seqs, GROUPS, NSTATE), HEADS // GROUPS, axis=1)
    step = jax.nn.softplus(step_pre + step_bias[None, :])
    decay = jnp.exp(-step * jnp.exp(decay_log)[None, :])
    x_heads = x_conv.reshape(seqs, HEADS, HEAD_DIM)
    new_state = (
        decay[:, :, None, None] * ssm_state + (step[:, :, None] * x_heads)[..., None] * in_map[:, :, None, :]
    )
    head_out = jnp.einsum("bhn,bhpn->bhp", out_map, new_state)
    head_out = head_out + skip_gain[None, :, None] * x_heads
    gated = head_out.reshape(seqs, HEADS * HEAD_DIM) * jax.nn.silu(z_pre.astype(jnp.float32))
    mixed = rms_norm(gated, inner_gain).astype(BF16)
    out = mix(
        ep, mixed.reshape(2, 32, LANES), xraw, r, ffn_gain.reshape(32, LANES), out_weight, expert_gate, expert_up,
        expert_down,
    )
    return out.reshape(seqs, width), new_state, new_conv_x, new_conv_bc


def solution(mesh):
    ep = mesh.shape["ep"]
    cols, rep = P(None, "ep"), P()
    placed = (
        P(GRP_EP, None), rep, cols, cols, cols, rep, rep, rep, rep, rep, rep,
        P(GRP_EP, None, None), P(GRP_EP, None, None), P(GRP_EP, None, None, None),
        rep, cols, rep, P("ep", None, None), P("ep", None, None), P("ep", None, None),
        P(GRP_EP, None), P(GRP_EP, None),
    )
    return jax.shard_map(
        functools.partial(body, ep),
        mesh=mesh,
        in_specs=placed,
        out_specs=(
            P(GRP_EP, None),
            P(GRP_EP, None, None, None),
            P(GRP_EP, None, None),
            P(GRP_EP, None, None),
        ),
        check_vma=False,
    )
```

time: 221 us -> 113 us (0.51)
  Pallas kernels: 0 us -> 90.6 us
  waiting for transfers between devices: 86.3 us -> 0 us
  blocking collectives: 68.5 us -> 0 us
  starting transfers between devices: 32.9 us -> 0 us
  matrix products: 13.9 us -> 3.38 us
    pallas_call x0 -> x2, Pallas kernels: none -> 90.6 us  [the longest x1 50.2 us: mix(): pl.pallas_call(functools.partial(mix_kernel, ep), out_shape=jax.ShapeDtyp...]
    all_to_all x4 -> x0, waiting for transfers between devices: 86.3 us -> none  [the longest x1 32 us: body(): lax.all_to_all(expert_rows, EP, split_axis=1, concat_axis=0, tiled=True)]
    all_to_all x1 -> x0, blocking collectives: 37.2 us -> none  [body(): lax.all_to_all(outgoing, EP, split_axis=0, concat_axis=1, tiled=True)]
    all_to_all x4 -> x0, starting transfers between devices: 32.9 us -> none  [the longest x1 18.5 us: copy_for_each(): return lax.all_to_all(copies, axis, split_axis=0, concat_axis=0, tiled=True)]
    all_gather x2 -> x0, blocking collectives: 31.3 us -> none  [gather_in_order(): tiles = lax.all_gather(tiles, axes[k], axis=0, tiled=True)]
    dot_general x9 -> x0, matrix products: 12.7 us -> none  [the longest x1 5.11 us: expert_apply(): jnp.einsum('erf,efd->erd', act, down_w, preferred_element_type=jnp.float32)]
    unnamed x27 -> x21, local copies, waits for them, and re-layouts: 2.04 us -> 6.08 us
  transfers between devices with their start and end apart: 4 -> 0, of which waited for: 4 -> 0; matrix products, arithmetic and copies ran while one was open for 2% -> 0% of each run, Pallas kernels for 0% -> 0%
where the time goes in v1:
time: 113 us
  Pallas kernels  90.6 us (80%)
  local copies, waits for them, and re-layouts  9.91 us (9%)
  other arithmetic  7.76 us (7%)
  matrix products  3.38 us (3%)
    pallas_call x1, Pallas kernels, mix(): pl.pallas_call(functools.partial(mix_kernel, ep), out_shape=jax.ShapeDtyp...  50.2 us
    pallas_call x1, Pallas kernels, project(): pl.pallas_call(functools.partial(project_kernel, ep), out_shape=(jax.Shap...  40.4 us
    unnamed x21, local copies, waits for them, and re-layouts  6.08 us
    add x1, other arithmetic, body(): decay[:, :, None, None] * ssm_state  5.91 us
    dot_general x1, matrix products, body(): head_out = jnp.einsum('bhn,bhpn->bhp', out_map, new_state)  3.38 us

profile of v1, /device:TPU:69, one launch (start us, length us, event | category | flops | bytes accessed | tf_op | source)
XLA Modules:
  0.0 112.5 jit_solution(9680443652836341754)
XLA Ops:
  0.6 0.0 copy-start.7
  0.6 0.0 copy-start.6
  0.7 0.0 copy-start.1
  0.7 0.0 copy-start
  0.7 0.0 copy-start.4
  0.7 0.0 copy-start.3
  0.7 2.3 %copy.28.wbc_hbm = bf16[4096,32]{1,0:T(8,128)(2,1)} copy(bf16[4096,32]{0,1:T(8,128)(2,1)} %param.26) | data formatting | bytes 524288 | tf_op args[4]
  3.0 2.4 %copy.29.wst_hbm = bf16[4096,64]{1,0:T(8,128)(2,1)} copy(bf16[4096,64]{0,1:T(8,128)(2,1)} %param.27) | data formatting | bytes 1048576 | tf_op args[5]
  5.4 1.3 %copy.37 = bf16[1,2,32,128]{3,2,1,0:T(8,128)(2,1)} copy(bf16[1,2,32,128]{3,1,2,0:T(2,128)(2,1)} %bitcast.46) | data formatting | bytes 32768
  6.7 40.4 %project.1 = (bf16[32,8,128]{2,1,0:T(8,128)(2,1)}, bf16[64,4096]{1,0:T(8,128)(2,1)}, f32[64,64]{1,0:T(8,128)}) custom-call(bf16[2,32,128]{2,1,0:T(8,128)(2,1)} %bitcast.42, f32[32,128]{1,0:T(8,128)} %bitcast.44, bf16[4096,128]{1,0:T(8,128)(2,1)} %wz_hbm.1, bf16[4096,128]{1,0:T(8,128)(2,1)} %wx_hbm.1, bf16[4096,32]{1,0:T(8,128)(2,1)} %copy.28.wbc_hbm, ...), custom_call_target="tpu_custom_call" | custom-call | tf_op jit(solution)/shard_map/project/pallas_call | solution.py:307
  47.1 0.0 copy-done.7
  47.1 0.0 copy-done.6
  47.2 0.7 multiply_exponential_fusion
  47.9 0.9 copy.30
  48.8 0.0 copy-done.1
  48.8 0.0 copy-done
  48.8 0.1 multiply_reduce_fusion
  48.9 0.1 reduce_sum.41
  49.0 0.1 broadcast_multiply_fusion
  49.2 0.0 copy-done.4
  49.2 0.0 copy-done.3
  49.3 5.9 %multiply_add_fusion = f32[2,64,64,128]{3,2,1,0:T(8,128)} fusion(f32[2,64,64,128]{3,2,1,0:T(8,128)} %param.35, f32[2,64,128]{2,1,0:T(8,128)S(1)} %bitcast.37, f32[2,64,64]{2,1,0:T(8,128)S(1)} %broadcast_multiply_fusion, f32[2,64]{1,0:T(2,128)S(1)} %get-tuple-element.12), kind=kLoop, calls=%fused_computation | loop fusion | flops 3145728 | bytes 8487424 | tf_op jit(solution)/shard_map/add | solution.py:403
  55.2 0.0 copy-start.5
  55.2 0.0 copy-start.2
  55.3 3.4 %fusion.1 = f32[2,64,1,64]{3,2,1,0:T(1,128)S(1)} fusion(f32[2,64,128,1]{2,3,1,0:T(1,128)S(1)} %bitcast.38, f32[2,64,64,128]{3,2,1,0:T(8,128)} %multiply_add_fusion), kind=kOutput, calls=%fused_computation.21 | convolution fusion | flops 2097152 | bytes 4292608 | tf_op jit(solution)/shard_map/bhn,bhpn->bhp/dot_general | solution.py:405
  58.6 0.1 reshape.100
  58.7 0.0 copy-done.5
  58.7 0.2 multiply_reduce_fusion.1
  58.9 0.1 reshape.97
  59.0 0.0 copy-done.2
  59.0 0.7 multiply_convert_fusion.mix_hbm
  59.7 50.2 %mix.1 = bf16[64,128]{1,0:T(8,128)(2,1)} custom-call(bf16[2,32,128]{2,1,0:T(8,128)(2,1)} %multiply_convert_fusion.mix_hbm, bf16[64,4096]{1,0:T(8,128)(2,1)} %get-tuple-element.9.xraw, bf16[32,8,128]{2,1,0:T(8,128)(2,1)} %get-tuple-element.7.r_in, f32[32,128]{1,0:T(8,128)} %bitcast.48, bf16[4096,128]{1,0:T(8,128)(2,1)} %wo_hbm.1, ...), custom_call_target="tpu_custom_call" | custom-call | tf_op jit(solution)/shard_map/mix/pallas_call | solution.py:336
  109.9 1.3 %reshape.99 = bf16[2,4096]{1,0:T(2,128)(2,1)} reshape(bf16[64,128]{1,0:T(8,128)(2,1)} %mix.1) | data formatting | bytes 32768 | tf_op jit(solution)/shard_map/reshape | solution.py:413
  111.3 0.7 slice.33
  111.9 0.6 slice.34
  (17 shorter events, 0.3 us)
Async XLA Ops:
  0.6 46.5 %copy-start.7 = (f32[64]{0:T(128)S(1)}, f32[64]{0:T(128)}, u32[]{:S(2)}) copy-start(f32[64]{0:T(128)} %param.29) | copy-start | bytes 772
  0.6 46.5 %copy-start.6 = (f32[64]{0:T(128)S(1)}, f32[64]{0:T(128)}, u32[]{:S(2)}) copy-start(f32[64]{0:T(128)} %param.28) | copy-start | bytes 772
  0.7 48.1 %copy-start.1 = (bf16[2,3,4096]{2,0,1:T(2,128)(2,1)S(1)}, bf16[2,3,4096]{2,0,1:T(2,128)(2,1)}, u32[]{:S(2)}) copy-start(bf16[2,3,4096]{2,0,1:T(2,128)(2,1)} %param.33) | copy-start | bytes 147460
  0.7 48.2 %copy-start = (f32[4,4096]{1,0:T(4,128)S(1)}, f32[4,4096]{1,0:T(4,128)}, u32[]{:S(2)}) copy-start(f32[4,4096]{1,0:T(4,128)} %param.31) | copy-start | bytes 196612
  0.7 48.5 %copy-start.4 = (bf16[2,3,1024]{2,0,1:T(2,128)(2,1)S(1)}, bf16[2,3,1024]{2,0,1:T(2,128)(2,1)}, u32[]{:S(2)}) copy-start(bf16[2,3,1024]{2,0,1:T(2,128)(2,1)} %param.34) | copy-start | bytes 36868
  0.7 48.5 %copy-start.3 = (f32[4,1024]{1,0:T(4,128)S(1)}, f32[4,1024]{1,0:T(4,128)}, u32[]{:S(2)}) copy-start(f32[4,1024]{1,0:T(4,128)} %param.32) | copy-start | bytes 49156
  55.2 3.5 %copy-start.5 = (f32[64]{0:T(128)S(1)}, f32[64]{0:T(128)}, u32[]{:S(2)}) copy-start(f32[64]{0:T(128)} %param.30) | copy-start | bytes 772
  55.2 3.8 %copy-start.2 = (f32[4096]{0:T(1024)S(1)}, f32[4096]{0:T(1024)}, u32[]{:S(2)}) copy-start(f32[4096]{0:T(1024)} %param.36) | copy-start | bytes 49156

commit v2 on v1

v2 whole, which is shorter than its diff:
```python
import functools

import jax
import jax.numpy as jnp
from jax import lax
from jax.experimental import pallas as pl
from jax.experimental.pallas import tpu as pltpu
from jax.sharding import PartitionSpec as P

TOPK = 4
GRP_EP = ("grp", "ep")
MESH = pl.DeviceIdType.MESH
F32 = jnp.float32
BF16 = jnp.bfloat16
LANES = 128
PITCH = 40

OWN = (6, -6, 3, -3, 1, -1)
RELAYS = (3, -3, 6, -6)


class Comm:
    def __init__(self, ep):
        self.ep = ep
        self.nz = ep // 2
        self.me = lax.axis_index("ep")
        self.core = lax.rem(self.me, 2)
        self.z = lax.div(self.me, 2)

    def at(self, offset, core):
        return lax.rem(self.z + offset + self.nz, self.nz) * 2 + core

    def partner(self):
        return self.z * 2 + (1 - self.core)

    def barrier(self):
        sem = pltpu.get_barrier_semaphore()

        def greet(i, carry):
            pl.semaphore_signal(
                sem, inc=1, device_id={"ep": lax.rem(self.me + i, self.ep)}, device_id_type=MESH
            )
            return carry

        lax.fori_loop(1, self.ep, greet, 0)
        return lambda: pl.semaphore_wait(sem, self.ep - 1)

    def copy(self, src, dst, send, recv, to):
        return pltpu.make_async_remote_copy(
            src_ref=src, dst_ref=dst, send_sem=send, recv_sem=recv, device_id={"ep": to}, device_id_type=MESH
        )

    def gather(self, buf, send, recv, landed):
        core, me = self.core, self.me

        def pass_on(block, to):
            self.copy(buf.at[block], buf.at[block], send, recv.at[block], to).start()

        def arrive(block):
            self.copy(buf.at[block], buf.at[block], send, recv.at[block], me).wait_recv()

        for d in OWN:
            pass_on(me, self.at(d, core))
        pass_on(me, self.partner())
        landed(me)
        extra = 2 - 4 * core
        for d in RELAYS:
            block = self.at(-d, core)
            arrive(block)
            pass_on(block, self.at(1, core))
            pass_on(block, self.at(-1, core))
            if d == 6:

                @pl.when(core == 0)
                def _(block=block):
                    pass_on(block, self.at(2, core))

            if d == -6:

                @pl.when(core == 1)
                def _(block=block):
                    pass_on(block, self.at(-2, core))

            pass_on(block, self.partner())
            landed(block)
        del extra
        for d in (1, -1, 2, -2, 4, -4, 5, -5, 7, -7, 8):
            block = self.at(-d, core)
            arrive(block)
            pass_on(block, self.partner())
            landed(block)

        def other(i, carry):
            block = self.at(i, 1 - core)
            arrive(block)
            landed(block)
            return carry

        lax.fori_loop(0, self.nz, other, 0)
        n = self.nz - 1 + self.nz
        whole = buf.at[pl.ds(0, n)]
        self.copy(whole, whole, send, recv.at[0], me).wait_send()

    def exchange(self, out, back, send, recv):
        me, ep, nz = self.me, self.ep, self.nz

        def one(to):
            self.copy(out.at[to], back.at[me], send, recv.at[me], to).start()

        def far_first(k, carry):
            offset = (nz // 2 - lax.div(k + 1, 2)) * (1 - 2 * lax.rem(k, 2))
            one(self.at(offset, 0))
            one(self.at(offset, 1))
            return carry

        lax.fori_loop(0, nz - 1, far_first, 0)
        one(self.partner())
        back[me] = out[me]

    def exchanged(self, out, back, send, recv, landed):
        me, ep = self.me, self.ep
        landed(me)

        def one(i, carry):
            frm = lax.rem(me + i, ep)
            self.copy(back.at[frm], back.at[frm], send, recv.at[frm], me).wait_recv()
            landed(frm)
            return carry

        lax.fori_loop(1, ep, one, 0)
        whole = out.at[pl.ds(0, ep - 1)]
        self.copy(whole, whole, send, recv.at[0], me).wait_send()


def tall(x, n):
    return x.reshape(n, x.shape[0] // n, x.shape[1])


def vmem():
    return pl.BlockSpec(memory_space=pltpu.VMEM)


def hbm():
    return pl.BlockSpec(memory_space=pl.ANY)


def smem():
    return pl.BlockSpec(memory_space=pltpu.SMEM)


def rows_of(dst, src, base):
    for j in range(src.shape[1] // LANES):
        dst[base + j : base + j + 1, :] = src[:, j * LANES : (j + 1) * LANES]


def row_of(dst, r, src, base, n):
    for j in range(n):
        dst[r : r + 1, j * LANES : (j + 1) * LANES] = src[base + j : base + j + 1, :]


def layer_kernel(
    ep, tok, mix_gain, wz_hbm, wx_hbm, wbc_hbm, wst_hbm, step_bias, decay_log, skip_gain, conv_x_w, conv_bc_w,
    conv_x, conv_bc, state_hbm, inner_gain, wo_hbm, ffn_gain, wg_hbm, wu_hbm, wd_hbm, routes, weights,
    out_ref, state_out, new_x, new_bc,
    buf, buf2, buf3, stage, lhs, xraw, wz, wx, wst, wo, wg, wu, wd, state, flat, out, back, tokf, convx, convbc,
    stepbc, decaybc, skipbc, bcs, ybuf, xbuf, rowx, rowbc, sq, act, wide, half_out, half_in, mine, total,
    send_rows, got_rows,
    wload, ssem, send1, recv1, send2, recv2, send3, recv3, hsend, hrecv, xsend, xrecv, csend, crecv,
):
    comm = Comm(ep)
    me, core = comm.me, comm.core
    ready = comm.barrier()
    pairs = (
        (wz_hbm, wz), (wx_hbm, wx), (wst_hbm, wst.at[pl.ds(0, 64)]), (wbc_hbm, wst.at[pl.ds(64, 32)]),
        (state_hbm, state), (wo_hbm, wo), (wg_hbm.at[0], wg), (wu_hbm.at[0], wu), (wd_hbm.at[0], wd),
    )
    pulls = [pltpu.make_async_copy(a, b, wload.at[i]) for i, (a, b) in enumerate(pairs)]
    for p in pulls:
        p.start()

    rows = tok[...].astype(F32)
    for r in range(2):
        rows_of(tokf, rows[r : r + 1, :], r * 32)
    buf[me] = tall(tokf[...], 2).astype(BF16)
    for conv, taps, dst, n in ((conv_x, conv_x_w, convx, 32), (conv_bc, conv_bc_w, convbc, 8)):
        old = conv[0].astype(F32) * taps[0:1, :]
        for c in range(1, 3):
            old = old + conv[c].astype(F32) * taps[c : c + 1, :]
        for r in range(2):
            rows_of(dst, old[r : r + 1, :], r * n)
        rows_of(dst, taps[3:4, :], 2 * n)
    lane = lax.broadcasted_iota(jnp.int32, (1, LANES), 1)
    dense = jnp.zeros((1, LANES), F32)
    for r in range(2):
        for k in range(TOPK):
            dense = dense + jnp.where(lane == routes[r, k] + 32 * r, weights[r, k], 0.0)
    high = dense.astype(BF16).astype(F32)
    flat[pl.ds(3, 32, stride=8), :] = jnp.broadcast_to(high, (32, LANES))
    flat[pl.ds(7, 32, stride=8), :] = jnp.broadcast_to(dense - high, (32, LANES))
    blank = jnp.zeros((1, 64), F32)

    def column(row):
        return jnp.transpose(jnp.broadcast_to(row, (LANES, LANES)))

    skipbc[...] = column(jnp.concatenate([skip_gain[...], blank], axis=1))
    sq[...] = jnp.zeros((64, LANES), F32)
    ready()

    def landed(block):
        both = buf[block].astype(F32)
        for r in range(2):
            stage[pl.ds(pl.multiple_of((block * 2 + r) * PITCH, 8), 32), :] = both[r]

    comm.gather(buf, send1, recv1, landed)
    square = jnp.zeros((64, LANES), F32)
    for j in range(32):
        x = stage[pl.ds(j, 64, stride=PITCH), :]
        square = square + x * x
        xraw[:, j * LANES : (j + 1) * LANES] = x.astype(BF16)
        lhs[:, j * LANES : (j + 1) * LANES] = (x * mix_gain[j : j + 1, :]).astype(BF16)
    scale = lax.rsqrt(jnp.sum(square, axis=1, keepdims=True) / 4096.0 + 1e-6)
    for p in pulls[:4]:
        p.wait()
    left = lhs[...]
    z = jnp.dot(left, wz[...], preferred_element_type=F32) * scale
    flat[pl.ds(0, 64, stride=4), :] = z
    x = jnp.dot(left, wx[...], preferred_element_type=F32) * scale
    flat[pl.ds(1, 64, stride=4), :] = x
    st = lax.dot_general(left, wst[...], (((1,), (1,)), ((), ())), preferred_element_type=F32) * scale
    bc = st[:, 64:96]
    spread = jnp.concatenate([bc, bc, bc, bc], axis=1)
    flat[pl.ds(2, 64, stride=4), :] = jnp.where(lax.div(lane, 32) == lax.rem(me, 4), spread, 0.0)
    out[...] = tall(flat[...], 32).astype(BF16)
    comm.exchange(out, back, xsend, xrecv)

    flat[pl.ds(0, 64, stride=4), :] = jnp.concatenate([st[:, 0:64], st[:, 0:64]], axis=1)
    mine8 = flat[pl.ds(pl.multiple_of(me * 8, 8), 8), :]
    bias = jnp.concatenate([step_bias[...], blank], axis=1)
    rate = jnp.exp(jnp.concatenate([decay_log[...], blank], axis=1))
    for r in range(2):
        step = jax.nn.softplus(mine8[r * 4 : r * 4 + 1, :] + bias)
        stepbc[pl.ds(r * LANES, LANES), :] = column(step)
        decaybc[pl.ds(r * LANES, LANES), :] = column(jnp.exp(-step * rate))
    comm.exchanged(out, back, xsend, xrecv, lambda frm: None)
    flat[...] = back[...].astype(F32).reshape(256, LANES)
    pulls[4].wait()

    low = lax.broadcasted_iota(jnp.int32, (32, LANES), 1) < 64
    for r in range(2):
        x_pre = flat[pl.ds(4 * r + 1, 32, stride=8), :]
        bc_pre = flat[pl.ds(4 * r + 2, 8, stride=32), :]
        for q in range(1, 4):
            bc_pre = bc_pre + flat[pl.ds(8 * q + 4 * r + 2, 8, stride=32), :]
        xbuf[pl.ds(r * 32, 32), :] = x_pre
        bcs[pl.ds(16 + r * 8, 8), :] = bc_pre
        xc = jax.nn.silu(convx[pl.ds(r * 32, 32), :] + convx[pl.ds(64, 32), :] * x_pre)
        bcs[pl.ds(r * 8, 8), :] = jax.nn.silu(convbc[pl.ds(r * 8, 8), :] + convbc[pl.ds(16, 8), :] * bc_pre)
        per = jnp.where(
            low,
            stepbc[pl.ds(r * LANES, 32, stride=2), :],
            stepbc[pl.ds(r * LANES + 1, 32, stride=2), :],
        )
        skip = jnp.where(low, skipbc[pl.ds(0, 32, stride=2), :], skipbc[pl.ds(1, 32, stride=2), :])
        total[pl.ds(r * 32, 32), :] = per * xc
        total[pl.ds(64 + r * 32, 32), :] = skip * xc

    def group(i, carry):
        r, g = lax.div(i, 4), lax.rem(i, 4)
        cols = jnp.transpose(total[pl.ds(pl.multiple_of(i * 8, 8), 8), :])
        into = jnp.broadcast_to(bcs[pl.ds(r * 8 + g, 1), :], (LANES, LANES))
        outof = jnp.broadcast_to(bcs[pl.ds(r * 8 + 4 + g, 1), :], (8, LANES)).astype(BF16)
        for k in range(8):
            h = g * 16 + 2 * k
            dec = jnp.concatenate(
                [
                    jnp.broadcast_to(decaybc[pl.ds(r * LANES + h, 1), :], (64, LANES)),
                    jnp.broadcast_to(decaybc[pl.ds(r * LANES + h + 1, 1), :], (64, LANES)),
                ],
                axis=0,
            )
            new = dec * state[r, pl.ds(h, 2)].reshape(LANES, LANES)
            new = new + jnp.broadcast_to(cols[:, k : k + 1], (LANES, LANES)) * into
            state[r, pl.ds(h, 2)] = new.reshape(2, 64, LANES)
            y = lax.dot_general(
                outof, new.astype(BF16), (((1,), (1,)), ((), ())), preferred_element_type=F32
            )
            ybuf[pl.ds(i * 8 + k, 1), :] = y[0:1, :]
        return carry

    lax.fori_loop(0, 8, group, 0)
    store = pltpu.make_async_copy(state, state_out, ssem)
    store.start()
    for r in range(2):
        at = pl.ds(r * 32, 32)
        gated = ybuf[at, :] + total[pl.ds(64 + r * 32, 32), :]
        gated = gated * jax.nn.silu(flat[pl.ds(4 * r, 32, stride=8), :])
        mean = jnp.sum(jnp.sum(gated * gated, axis=1, keepdims=True), axis=0, keepdims=True) / 4096.0
        buf2[me, r] = (gated * lax.rsqrt(mean + 1e-6) * inner_gain[...]).astype(BF16)

    def landed2(block):
        both = buf2[block].astype(F32)
        for r in range(2):
            stage[pl.ds(pl.multiple_of((block * 2 + r) * PITCH, 8), 32), :] = both[r]

    comm.gather(buf2, send2, recv2, landed2)
    for j in range(32):
        lhs[:, j * LANES : (j + 1) * LANES] = stage[pl.ds(j, 64, stride=PITCH), :].astype(BF16)
    pulls[5].wait()
    buf3[me] = jnp.dot(lhs[...], wo[...], preferred_element_type=F32).astype(BF16)

    def landed3(block):
        cols = pl.ds(pl.multiple_of(block * LANES, LANES), LANES)
        resid = (xraw[:, cols].astype(F32) + buf3[block].astype(F32)).astype(BF16).astype(F32)
        sq[...] = sq[...] + resid * resid
        stage[pl.ds(block, 64, stride=PITCH), :] = resid
        lhs[:, cols] = (resid * ffn_gain[pl.ds(block, 1), :]).astype(BF16)

    comm.gather(buf3, send3, recv3, landed3)
    scale = lax.rsqrt(jnp.sum(sq[...], axis=1, keepdims=True) / 4096.0 + 1e-6)
    pulls[6].wait()
    pulls[7].wait()
    left = lhs[...]
    gate = jnp.dot(left, wg[...], preferred_element_type=F32) * scale
    up = jnp.dot(left, wu[...], preferred_element_type=F32) * scale
    act[...] = (jax.nn.silu(gate) * up).astype(BF16)
    pulls[8].wait()
    lanes32 = lax.broadcasted_iota(jnp.int32, (32, LANES), 1)
    dense = flat[pl.ds(3, 32, stride=8), :] + flat[pl.ds(7, 32, stride=8), :]
    for r in range(2):
        picked = jnp.sum(jnp.where(lanes32 == me + 32 * r, dense, 0.0), axis=1, keepdims=True)
        wide[pl.ds(r, 32, stride=2), :] = jnp.broadcast_to(picked, (32, LANES))
    weight = jnp.concatenate([wide[...]] * 4, axis=1)

    def expert(half, k):
        cols = pl.ds(pl.multiple_of(half * 2048 + k * 512, 512), 512)
        y = jnp.dot(act[...], wd[:, cols], preferred_element_type=F32).astype(BF16).astype(F32)
        return y * weight

    for k in range(4):
        half_out[:, k * 512 : (k + 1) * 512] = expert(1 - core, k).astype(BF16)
    swap = comm.copy(half_out, half_in, hsend, hrecv, comm.partner())
    swap.start()
    for k in range(4):
        mine[:, k * 512 : (k + 1) * 512] = expert(core, k)
    swap.wait()
    for j in range(16):
        cols = slice(j * LANES, (j + 1) * LANES)
        total[pl.ds(j, 64, stride=24), :] = mine[:, cols] + half_in[:, cols].astype(F32)

    def pack(t, carry):
        for r in range(2):
            send_rows[t, r] = total[pl.ds(pl.multiple_of((t * 2 + r) * 24, 8), 16), :].astype(BF16)
        return carry

    lax.fori_loop(0, ep, pack, 0)
    comm.exchange(send_rows, got_rows, csend, crecv)
    for r in range(2):
        tokf[pl.ds(r * 32, 32), :] = stage[pl.ds(pl.multiple_of((me * 2 + r) * PITCH, 8), 32), :]
    for r in range(2):
        row_of(rowx, r, xbuf, r * 32, 32)
        row_of(rowbc, r, bcs, 16 + r * 8, 8)
    for old, new, row in ((conv_x, new_x, rowx), (conv_bc, new_bc, rowbc)):
        new[0] = old[1]
        new[1] = old[2]
        new[2] = row[...].astype(BF16)

    def arrived(frm):
        h = lax.rem(frm, 2)
        for r in range(2):
            at = pl.ds(pl.multiple_of(r * 32 + h * 16, 8), 16)
            tokf[at, :] = tokf[at, :] + got_rows[frm, r].astype(F32)

    comm.exchanged(send_rows, got_rows, csend, crecv, arrived)
    for r in range(2):
        row_of(rowx, r, tokf, r * 32, 32)
    out_ref[...] = rowx[...].astype(BF16)
    store.wait()


def layer(ep, *args):
    dma = pltpu.SemaphoreType.DMA
    v = pltpu.VMEM
    state = args[13]
    return pl.pallas_call(
        functools.partial(layer_kernel, ep),
        out_shape=(
            jax.ShapeDtypeStruct((2, 4096), BF16),
            jax.ShapeDtypeStruct(state.shape, F32),
            jax.ShapeDtypeStruct(args[11].shape, BF16),
            jax.ShapeDtypeStruct(args[12].shape, BF16),
        ),
        in_specs=[
            vmem(), vmem(), hbm(), hbm(), hbm(), hbm(), vmem(), vmem(), vmem(), vmem(), vmem(),
            vmem(), vmem(), hbm(), vmem(), hbm(), vmem(), hbm(), hbm(), hbm(), smem(), smem(),
        ],
        out_specs=(vmem(), hbm(), vmem(), vmem()),
        scratch_shapes=[
            v((ep, 2, 32, LANES), BF16), v((ep, 2, 32, LANES), BF16), v((ep, 64, LANES), BF16),
            v((64 * PITCH, LANES), F32), v((64, 4096), BF16), v((64, 4096), BF16),
            v((4096, LANES), BF16), v((4096, LANES), BF16), v((96, 4096), BF16), v((4096, LANES), BF16),
            v((4096, 512), BF16), v((4096, 512), BF16), v((512, 4096), BF16), v(state.shape, F32),
            v((256, LANES), F32), v((ep, 8, LANES), BF16), v((ep, 8, LANES), BF16), v((64, LANES), F32),
            v((96, LANES), F32), v((24, LANES), F32),
            v((256, LANES), F32), v((256, LANES), F32), v((LANES, LANES), F32), v((32, LANES), F32),
            v((64, LANES), F32), v((64, LANES), F32), v((2, 4096), F32), v((2, 1024), F32), v((64, LANES), F32),
            v((64, 512), BF16), v((64, LANES), F32), v((64, 2048), BF16), v((64, 2048), BF16),
            v((64, 2048), F32), v((64 * 24, LANES), F32),
            v((ep, 2, 16, LANES), BF16), v((ep, 2, 16, LANES), BF16),
            dma((9,)), dma, dma, dma((ep,)), dma, dma((ep,)), dma, dma((ep,)), dma, dma, dma, dma((ep,)),
            dma, dma((ep,)),
        ],
        compiler_params=pltpu.CompilerParams(collective_id=0, has_side_effects=True),
        name="layer",
    )(*args)


def body(
    ep, tokens_in, mix_gain, w_gate_z, w_value, w_in_bc, w_step, step_bias, decay_log, skip_gain, conv_x_weight,
    conv_bc_weight, conv_x_state, conv_bc_state, ssm_state, inner_gain, out_weight, ffn_gain, expert_gate,
    expert_up, expert_down, routes, route_weight,
):
    out, new_state, new_x, new_bc = layer(
        ep, tokens_in, mix_gain.reshape(32, LANES), w_gate_z, w_value, w_in_bc.T, w_step.T,
        step_bias.reshape(1, 64), decay_log.reshape(1, 64), skip_gain.reshape(1, 64), conv_x_weight,
        conv_bc_weight, conv_x_state.transpose(1, 0, 2), conv_bc_state.transpose(1, 0, 2), ssm_state,
        inner_gain.reshape(32, LANES), out_weight, ffn_gain.reshape(32, LANES), expert_gate, expert_up,
        expert_down, routes, route_weight,
    )
    return out, new_state, new_x.transpose(1, 0, 2), new_bc.transpose(1, 0, 2)


def solution(mesh):
    ep = mesh.shape["ep"]
    cols, rep = P(None, "ep"), P()
    placed = (
        P(GRP_EP, None), rep, cols, cols, cols, rep, rep, rep, rep, rep, rep,
        P(GRP_EP, None, None), P(GRP_EP, None, None), P(GRP_EP, None, None, None),
        rep, cols, rep, P("ep", None, None), P("ep", None, None), P("ep", None, None),
        P(GRP_EP, None), P(GRP_EP, None),
    )
    return jax.shard_map(
        functools.partial(body, ep),
        mesh=mesh,
        in_specs=placed,
        out_specs=(
            P(GRP_EP, None),
            P(GRP_EP, None, None, None),
            P(GRP_EP, None, None),
            P(GRP_EP, None, None),
        ),
        check_vma=False,
    )
```

time: 113 us -> 96.3 us (0.85)
  other arithmetic: 7.76 us -> 0 us
  matrix products: 3.38 us -> 0 us
  local copies, waits for them, and re-layouts: 9.91 us -> 7.36 us
  Pallas kernels: 90.6 us -> 88.1 us
    add x1 -> x0, other arithmetic: 5.91 us -> none  [body(): decay[:, :, None, None] * ssm_state]
    dot_general x1 -> x0, matrix products: 3.38 us -> none  [body(): head_out = jnp.einsum('bhn,bhpn->bhp', out_map, new_state)]
    pallas_call x2 -> x1, Pallas kernels: 90.6 us -> 88.1 us  [layer(): pl.pallas_call(functools.partial(layer_kernel, ep), out_shape=(jax.ShapeD...]
    reshape x4 -> x0, local copies, waits for them, and re-layouts: 1.44 us -> none  [the longest x1 1.33 us: body(): return (out.reshape(seqs, width), new_state, new_conv_x, new_conv_bc)]
    unnamed x21 -> x8, local copies, waits for them, and re-layouts: 6.08 us -> 7.36 us
    slice x3 -> x0, local copies, waits for them, and re-layouts: 1.27 us -> none  [the longest x2 1.26 us: conv_step(): return (mixed, window[:, 1:])]
where the time goes in v2:
time: 96.3 us; the launch traced here: 96.1 us
  Pallas kernels  88.1 us (91%)
  local copies, waits for them, and re-layouts  7.36 us (8%)
    pallas_call x1, Pallas kernels, layer(): pl.pallas_call(functools.partial(layer_kernel, ep), out_shape=(jax.ShapeD...  88.1 us
    unnamed x8, local copies, waits for them, and re-layouts  7.36 us

profile of v2, /device:TPU:69, one launch (start us, length us, event | category | flops | bytes accessed | tf_op | source)
XLA Modules:
  0.0 96.1 jit_solution(17564655928220390634)
XLA Ops:
  0.6 88.1 %layer.1 = (bf16[2,4096]{1,0:T(2,128)(2,1)}, f32[2,64,64,128]{3,2,1,0:T(8,128)}, bf16[3,2,4096]{2,1,0:T(2,128)(2,1)}, bf16[3,2,1024]{2,1,0:T(2,128)(2,1)}) custom-call(bf16[2,4096]{1,0:T(2,128)(2,1)} %tok.1, f32[32,128]{1,0:T(8,128)} %bitcast.16, bf16[4096,128]{1,0:T(8,128)(2,1)} %wz_hbm.1, bf16[4096,128]{1,0:T(8,128)(2,1)} %wx_hbm.1, ...), custom_call_target="tpu_custom_call" | custom-call | tf_op jit(solution)/shard_map/layer/pallas_call | solution.py:384
  88.7 1.3 %copy.30 = bf16[2,4096]{1,0:T(2,128)(2,1)} copy(bf16[2,4096]{1,0:T(2,128)(2,1)} %get-tuple-element.16) | data formatting | bytes 32768
  90.1 0.0 copy-start
  90.1 0.0 copy-start.1
  90.1 4.8 %copy.31 = f32[2,64,64,128]{3,2,1,0:T(8,128)} copy(f32[2,64,64,128]{3,2,1,0:T(8,128)} %get-tuple-element.17) | data formatting | bytes 8388608
  94.8 0.0 copy-done
  94.9 0.6 copy.32
  95.5 0.0 copy-done.1
  95.5 0.6 copy.33
Async XLA Ops:
  90.1 4.8 %copy-start = (bf16[3,2,4096]{2,1,0:T(2,128)(2,1)S(1)}, bf16[3,2,4096]{2,1,0:T(2,128)(2,1)}, u32[]{:S(2)}) copy-start(bf16[3,2,4096]{2,1,0:T(2,128)(2,1)} %get-tuple-element.10) | copy-start | bytes 147460
  90.1 5.4 %copy-start.1 = (bf16[3,2,1024]{2,1,0:T(2,128)(2,1)S(1)}, bf16[3,2,1024]{2,1,0:T(2,128)(2,1)}, u32[]{:S(2)}) copy-start(bf16[3,2,1024]{2,1,0:T(2,128)(2,1)} %get-tuple-element.11) | copy-start | bytes 36868

commit v3 on v2

--- a/solution.py
+++ b/solution.py
@@ -14,9 +14,11 @@
 BF16 = jnp.bfloat16
 LANES = 128
 PITCH = 40
+VMEM_LIMIT = 34 * 1024 * 1024
 
 OWN = (6, -6, 3, -3, 1, -1)
-RELAYS = (3, -3, 6, -6)
+RELAYS = ((3, (1, -1)), (-3, (1, -1)), (6, (2, 1, -1)), (-6, (1, -1)))
+LEAVES = (1, -1, 2, -2, 4, -4, 5, -5, 7, -7, 8)
 
 
 class Comm:
@@ -59,47 +61,47 @@
         def arrive(block):
             self.copy(buf.at[block], buf.at[block], send, recv.at[block], me).wait_recv()
 
+        def sent(n):
+            whole = buf.at[pl.ds(0, n)]
+            self.copy(whole, whole, send, recv.at[0], me).wait_send()
+
+        def turned(d, side):
+            return d if side == 0 else -d
+
         for d in OWN:
-            pass_on(me, self.at(d, core))
+            pass_on(me, self.at(d * (1 - 2 * core), 1))
         pass_on(me, self.partner())
         landed(me)
-        extra = 2 - 4 * core
-        for d in RELAYS:
-            block = self.at(-d, core)
-            arrive(block)
-            pass_on(block, self.at(1, core))
-            pass_on(block, self.at(-1, core))
-            if d == 6:
-
-                @pl.when(core == 0)
-                def _(block=block):
-                    pass_on(block, self.at(2, core))
-
-            if d == -6:
-
-                @pl.when(core == 1)
-                def _(block=block):
-                    pass_on(block, self.at(-2, core))
-
-            pass_on(block, self.partner())
-            landed(block)
-        del extra
-        for d in (1, -1, 2, -2, 4, -4, 5, -5, 7, -7, 8):
-            block = self.at(-d, core)
-            arrive(block)
-            pass_on(block, self.partner())
-            landed(block)
-
-        def other(i, carry):
-            block = self.at(i, 1 - core)
-            arrive(block)
-            landed(block)
-            return carry
-
-        lax.fori_loop(0, self.nz, other, 0)
-        n = self.nz - 1 + self.nz
-        whole = buf.at[pl.ds(0, n)]
-        self.copy(whole, whole, send, recv.at[0], me).wait_send()
+        steps = RELAYS + tuple((d, ()) for d in LEAVES)
+
+        @pl.when(core == 1)
+        def _():
+            passed = 0
+            for d, onward in steps:
+                for side in range(2):
+                    block = self.at(-turned(d, side), side)
+                    arrive(block)
+                    for step in onward:
+                        pass_on(block, self.at(turned(step, side), 1))
+                    pass_on(block, self.partner())
+                    passed += len(onward) + 1
+                    landed(block)
+            arrive(self.partner())
+            landed(self.partner())
+            sent(len(OWN) + 1)
+            for start in range(0, passed, self.ep):
+                sent(min(self.ep, passed - start))
+
+        @pl.when(core == 0)
+        def _():
+            arrive(self.partner())
+            landed(self.partner())
+            for d, _ in steps:
+                for side in range(2):
+                    block = self.at(-turned(d, side), side)
+                    arrive(block)
+                    landed(block)
+            sent(len(OWN) + 1)
 
     def exchange(self, out, back, send, recv):
         me, ep, nz = self.me, self.ep, self.nz
@@ -158,30 +160,47 @@
         dst[r : r + 1, j * LANES : (j + 1) * LANES] = src[base + j : base + j + 1, :]
 
 
-def layer_kernel(
-    ep, tok, mix_gain, wz_hbm, wx_hbm, wbc_hbm, wst_hbm, step_bias, decay_log, skip_gain, conv_x_w, conv_bc_w,
-    conv_x, conv_bc, state_hbm, inner_gain, wo_hbm, ffn_gain, wg_hbm, wu_hbm, wd_hbm, routes, weights,
-    out_ref, state_out, new_x, new_bc,
-    buf, buf2, buf3, stage, lhs, xraw, wz, wx, wst, wo, wg, wu, wd, state, flat, out, back, tokf, convx, convbc,
-    stepbc, decaybc, skipbc, bcs, ybuf, xbuf, rowx, rowbc, sq, act, wide, half_out, half_in, mine, total,
-    send_rows, got_rows,
-    wload, ssem, send1, recv1, send2, recv2, send3, recv3, hsend, hrecv, xsend, xrecv, csend, crecv,
-):
+def layer_kernel(ep, n_in, n_out, *refs):
+    inputs, outputs, locals_, refs = (
+        refs[:n_in], refs[n_in : n_in + n_out], refs[n_in + n_out : 2 * n_in + n_out - 1], refs[2 * n_in + n_out - 1 :]
+    )
+    (
+        tok, mix_gain, wz, wx, wst, step_bias, decay_log, skip_gain, conv_x_w, conv_bc_w, conv_x, conv_bc, _,
+        inner_gain, wo, ffn_gain, wg, wu, wd, routes, weights,
+    ) = locals_
+    out_ref, state, new_x, new_bc = outputs
+    (
+        buf, buf2, buf3, stage, lhs, xraw, flat, out, back, tokf, convx, convbc,
+        stepbc, decaybc, skipbc, bcs, ybuf, xbuf, rowx, rowbc, sq, act, wide, half_out, half_in, mine, total,
+        send_rows, got_rows,
+        wload, send1, recv1, send2, recv2, send3, recv3, hsend, hrecv, xsend, xrecv, csend, crecv,
+    ) = refs
     comm = Comm(ep)
     me, core = comm.me, comm.core
     ready = comm.barrier()
+    (
+        tok_h, mix_h, wz_h, wx_h, wbc_h, wst_h, bias_h, decay_h, skip_h, cxw_h, cbw_h, cx_h, cb_h, state_h, inner_h,
+        wo_h, ffn_h, wg_h, wu_h, wd_h, routes_h, weights_h,
+    ) = inputs
     pairs = (
-        (wz_hbm, wz), (wx_hbm, wx), (wst_hbm, wst.at[pl.ds(0, 64)]), (wbc_hbm, wst.at[pl.ds(64, 32)]),
-        (state_hbm, state), (wo_hbm, wo), (wg_hbm.at[0], wg), (wu_hbm.at[0], wu), (wd_hbm.at[0], wd),
+        (tok_h, tok), (cx_h, conv_x), (cxw_h, conv_x_w), (cb_h, conv_bc), (cbw_h, conv_bc_w), (routes_h, routes),
+        (weights_h, weights), (skip_h, skip_gain), (bias_h, step_bias), (decay_h, decay_log), (mix_h, mix_gain),
+        (inner_h, inner_gain), (ffn_h, ffn_gain),
+        (wz_h, wz), (wx_h, wx), (wst_h, wst.at[pl.ds(0, 64)]), (wbc_h, wst.at[pl.ds(64, 32)]),
+        (state_h, state), (wo_h, wo), (wg_h.at[0], wg), (wu_h.at[0], wu), (wd_h.at[0], wd),
     )
     pulls = [pltpu.make_async_copy(a, b, wload.at[i]) for i, (a, b) in enumerate(pairs)]
     for p in pulls:
         p.start()
+    early, pulls = pulls[:13], pulls[13:]
+    early[0].wait()
 
     rows = tok[...].astype(F32)
     for r in range(2):
         rows_of(tokf, rows[r : r + 1, :], r * 32)
     buf[me] = tall(tokf[...], 2).astype(BF16)
+    for p in early[1:]:
+        p.wait()
     for conv, taps, dst, n in ((conv_x, conv_x_w, convx, 32), (conv_bc, conv_bc_w, convbc, 8)):
         old = conv[0].astype(F32) * taps[0:1, :]
         for c in range(1, 3):
@@ -212,21 +231,26 @@
             stage[pl.ds(pl.multiple_of((block * 2 + r) * PITCH, 8), 32), :] = both[r]
 
     comm.gather(buf, send1, recv1, landed)
-    square = jnp.zeros((64, LANES), F32)
-    for j in range(32):
-        x = stage[pl.ds(j, 64, stride=PITCH), :]
-        square = square + x * x
-        xraw[:, j * LANES : (j + 1) * LANES] = x.astype(BF16)
-        lhs[:, j * LANES : (j + 1) * LANES] = (x * mix_gain[j : j + 1, :]).astype(BF16)
-    scale = lax.rsqrt(jnp.sum(square, axis=1, keepdims=True) / 4096.0 + 1e-6)
     for p in pulls[:4]:
         p.wait()
-    left = lhs[...]
-    z = jnp.dot(left, wz[...], preferred_element_type=F32) * scale
+    square = jnp.zeros((64, LANES), F32)
+    z, x, st = jnp.zeros((64, LANES), F32), jnp.zeros((64, LANES), F32), jnp.zeros((64, 96), F32)
+    for k in range(16):
+        part = []
+        for j in (2 * k, 2 * k + 1):
+            chunk = stage[pl.ds(j, 64, stride=PITCH), :]
+            square = square + chunk * chunk
+            xraw[:, j * LANES : (j + 1) * LANES] = chunk.astype(BF16)
+            part.append((chunk * mix_gain[j : j + 1, :]).astype(BF16))
+        part = jnp.concatenate(part, axis=1)
+        at = slice(k * 256, (k + 1) * 256)
+        z = z + jnp.dot(part, wz[at, :], preferred_element_type=F32)
+        x = x + jnp.dot(part, wx[at, :], preferred_element_type=F32)
+        st = st + lax.dot_general(part, wst[:, at], (((1,), (1,)), ((), ())), preferred_element_type=F32)
+    scale = lax.rsqrt(jnp.sum(square, axis=1, keepdims=True) / 4096.0 + 1e-6)
+    z, x, st = z * scale, x * scale, st * scale
     flat[pl.ds(0, 64, stride=4), :] = z
-    x = jnp.dot(left, wx[...], preferred_element_type=F32) * scale
     flat[pl.ds(1, 64, stride=4), :] = x
-    st = lax.dot_general(left, wst[...], (((1,), (1,)), ((), ())), preferred_element_type=F32) * scale
     bc = st[:, 64:96]
     spread = jnp.concatenate([bc, bc, bc, bc], axis=1)
     flat[pl.ds(2, 64, stride=4), :] = jnp.where(lax.div(lane, 32) == lax.rem(me, 4), spread, 0.0)
@@ -288,8 +312,6 @@
         return carry
 
     lax.fori_loop(0, 8, group, 0)
-    store = pltpu.make_async_copy(state, state_out, ssem)
-    store.start()
     for r in range(2):
         at = pl.ds(r * 32, 32)
         gated = ybuf[at, :] + total[pl.ds(64 + r * 32, 32), :]
@@ -303,10 +325,13 @@
             stage[pl.ds(pl.multiple_of((block * 2 + r) * PITCH, 8), 32), :] = both[r]
 
     comm.gather(buf2, send2, recv2, landed2)
-    for j in range(32):
-        lhs[:, j * LANES : (j + 1) * LANES] = stage[pl.ds(j, 64, stride=PITCH), :].astype(BF16)
     pulls[5].wait()
-    buf3[me] = jnp.dot(lhs[...], wo[...], preferred_element_type=F32).astype(BF16)
+    cols_out = jnp.zeros((64, LANES), F32)
+    for k in range(16):
+        part = [stage[pl.ds(j, 64, stride=PITCH), :].astype(BF16) for j in (2 * k, 2 * k + 1)]
+        part = jnp.concatenate(part, axis=1)
+        cols_out = cols_out + jnp.dot(part, wo[k * 256 : (k + 1) * 256, :], preferred_element_type=F32)
+    buf3[me] = cols_out.astype(BF16)
 
     def landed3(block):
         cols = pl.ds(pl.multiple_of(block * LANES, LANES), LANES)
@@ -374,31 +399,31 @@
     for r in range(2):
         row_of(rowx, r, tokf, r * 32, 32)
     out_ref[...] = rowx[...].astype(BF16)
-    store.wait()
 
 
 def layer(ep, *args):
     dma = pltpu.SemaphoreType.DMA
     v = pltpu.VMEM
-    state = args[13]
-    return pl.pallas_call(
-        functools.partial(layer_kernel, ep),
-        out_shape=(
-            jax.ShapeDtypeStruct((2, 4096), BF16),
-            jax.ShapeDtypeStruct(state.shape, F32),
-            jax.ShapeDtypeStruct(args[11].shape, BF16),
-            jax.ShapeDtypeStruct(args[12].shape, BF16),
-        ),
-        in_specs=[
-            vmem(), vmem(), hbm(), hbm(), hbm(), hbm(), vmem(), vmem(), vmem(), vmem(), vmem(),
-            vmem(), vmem(), hbm(), vmem(), hbm(), vmem(), hbm(), hbm(), hbm(), smem(), smem(),
-        ],
-        out_specs=(vmem(), hbm(), vmem(), vmem()),
+    local = [v(a.shape[1:] if a.shape[0] == 1 and a.ndim == 3 else a.shape, a.dtype) for a in args]
+    local[4:6] = [v((96, 4096), BF16)]
+    del local[12]
+    local.insert(12, v((8, LANES), F32))
+    local[-2:] = [pltpu.SMEM(a.shape, a.dtype) for a in args[-2:]]
+    outs = (
+        jax.ShapeDtypeStruct((2, 4096), BF16),
+        jax.ShapeDtypeStruct(args[13].shape, F32),
+        jax.ShapeDtypeStruct(args[11].shape, BF16),
+        jax.ShapeDtypeStruct(args[12].shape, BF16),
+    )
+    results = pl.pallas_call(
+        functools.partial(layer_kernel, ep, len(args), len(outs)),
+        out_shape=outs,
+        in_specs=[hbm()] * len(args),
+        out_specs=(vmem(),) * len(outs),
         scratch_shapes=[
+            *local,
             v((ep, 2, 32, LANES), BF16), v((ep, 2, 32, LANES), BF16), v((ep, 64, LANES), BF16),
             v((64 * PITCH, LANES), F32), v((64, 4096), BF16), v((64, 4096), BF16),
-            v((4096, LANES), BF16), v((4096, LANES), BF16), v((96, 4096), BF16), v((4096, LANES), BF16),
-            v((4096, 512), BF16), v((4096, 512), BF16), v((512, 4096), BF16), v(state.shape, F32),
             v((256, LANES), F32), v((ep, 8, LANES), BF16), v((ep, 8, LANES), BF16), v((64, LANES), F32),
             v((96, LANES), F32), v((24, LANES), F32),
             v((256, LANES), F32), v((256, LANES), F32), v((LANES, LANES), F32), v((32, LANES), F32),
@@ -406,12 +431,32 @@
             v((64, 512), BF16), v((64, LANES), F32), v((64, 2048), BF16), v((64, 2048), BF16),
             v((64, 2048), F32), v((64 * 24, LANES), F32),
             v((ep, 2, 16, LANES), BF16), v((ep, 2, 16, LANES), BF16),
-            dma((9,)), dma, dma, dma((ep,)), dma, dma((ep,)), dma, dma((ep,)), dma, dma, dma, dma((ep,)),
+            dma((22,)), dma, dma((ep,)), dma, dma((ep,)), dma, dma((ep,)), dma, dma, dma, dma((ep,)),
             dma, dma((ep,)),
         ],
-        compiler_params=pltpu.CompilerParams(collective_id=0, has_side_effects=True),
+        compiler_params=pltpu.CompilerParams(
+            collective_id=0, has_side_effects=True, vmem_limit_bytes=VMEM_LIMIT
+        ),
         name="layer",
-    )(*args)
+    )(*(pltpu.with_memory_space_constraint(a, pltpu.HBM) for a in args))
+    return pl.pallas_call(
+        flush_kernel,
+        out_shape=outs,
+        in_specs=[vmem()] * len(outs),
+        out_specs=(hbm(),) * len(outs),
+        scratch_shapes=[dma((len(outs),))],
+        compiler_params=pltpu.CompilerParams(vmem_limit_bytes=1024 * 1024),
+        name="flush",
+    )(*results)
+
+
+def flush_kernel(*refs):
+    n = len(refs) // 2
+    copies = [pltpu.make_async_copy(refs[i], refs[n + i], refs[-1].at[i]) for i in range(n)]
+    for c in copies:
+        c.start()
+    for c in copies:
+        c.wait()
 
 
 def body(

time: 96.3 us -> 86.8 us (0.901)
  local copies, waits for them, and re-layouts: 7.36 us -> 0 us
  Pallas kernels: 88.1 us -> 86 us
    unnamed x8 -> x0, local copies, waits for them, and re-layouts: 7.36 us -> none
    pallas_call x1 -> x2, Pallas kernels: 88.1 us -> 86 us  [the longest x1 83.9 us: layer(): pl.pallas_call(functools.partial(layer_kernel, ep, len(args), len(outs)),...]
where the time goes in v3:
time: 86.8 us; the launch traced here: 86.6 us
  Pallas kernels  86 us (99%)
    pallas_call x1, Pallas kernels, layer(): pl.pallas_call(functools.partial(layer_kernel, ep, len(args), len(outs)),...  83.9 us
    pallas_call x1, Pallas kernels, layer(): pl.pallas_call(flush_kernel, out_shape=outs, in_specs=[vmem()] * len(outs...  2.06 us

profile of v3, /device:TPU:69, one launch (start us, length us, event | category | flops | bytes accessed | tf_op | source)
XLA Modules:
  0.0 86.6 jit_solution(6997151389952827169)
XLA Ops:
  0.6 83.9 %layer.1 = (bf16[2,4096]{1,0:T(2,128)(2,1)S(1)}, f32[2,64,64,128]{3,2,1,0:T(8,128)S(1)}, bf16[3,2,4096]{2,1,0:T(2,128)(2,1)S(1)}, bf16[3,2,1024]{2,1,0:T(2,128)(2,1)S(1)}) custom-call(bf16[2,4096]{1,0:T(2,128)(2,1)} %refs_0_.1, f32[32,128]{1,0:T(8,128)} %bitcast.15, bf16[4096,128]{1,0:T(8,128)(2,1)} %refs_2_.1, bf16[4096,128]{1,0:T(8,128)(2,1)} %refs_3_.1, ...), custom_call_target="tpu_custom_call" | custom-call | tf_op jit(solution)/shard_map/layer/pallas_call | solution.py:418
  84.6 2.1 %flush.1 = (bf16[2,4096]{1,0:T(2,128)(2,1)}, f32[2,64,64,128]{3,2,1,0:T(8,128)}, bf16[3,2,4096]{2,1,0:T(2,128)(2,1)}, bf16[3,2,1024]{2,1,0:T(2,128)(2,1)}) custom-call(bf16[2,4096]{1,0:T(2,128)(2,1)S(1)} %get-tuple-element.12.refs_0_, f32[2,64,64,128]{3,2,1,0:T(8,128)S(1)} %get-tuple-element.13.refs_1_, bf16[3,2,4096]{2,1,0:T(2,128)(2,1)S(1)} %get-tuple-element.14.refs_2_, ...), custom_call_target="tpu_custom_call" | custom-call | tf_op jit(solution)/shard_map/flush/pallas_call | solution.py:442

commit v4 on v3

--- a/solution.py
+++ b/solution.py
@@ -14,10 +14,11 @@
 BF16 = jnp.bfloat16
 LANES = 128
 PITCH = 40
-VMEM_LIMIT = 34 * 1024 * 1024
+VMEM_LIMIT = 38 * 1024 * 1024
 
 OWN = (6, -6, 3, -3, 1, -1)
 RELAYS = ((3, (1, -1)), (-3, (1, -1)), (6, (2, 1, -1)), (-6, (1, -1)))
+GREET = (1, -1, 2, -2, 3, -3, 6, -6)
 LEAVES = (1, -1, 2, -2, 4, -4, 5, -5, 7, -7, 8)
 
 
@@ -38,20 +39,28 @@
     def barrier(self):
         sem = pltpu.get_barrier_semaphore()
 
-        def greet(i, carry):
-            pl.semaphore_signal(
-                sem, inc=1, device_id={"ep": lax.rem(self.me + i, self.ep)}, device_id_type=MESH
-            )
-            return carry
-
-        lax.fori_loop(1, self.ep, greet, 0)
-        return lambda: pl.semaphore_wait(sem, self.ep - 1)
+        def greet(to):
+            pl.semaphore_signal(sem, inc=1, device_id={"ep": to}, device_id_type=MESH)
+
+        @pl.when(self.core == 1)
+        def _():
+            for d in GREET:
+                greet(self.at(d, 0))
+                greet(self.at(d, 1))
+
+        greet(self.partner())
+        return lambda: pl.semaphore_wait(sem, len(GREET) + 1)
 
     def copy(self, src, dst, send, recv, to):
         return pltpu.make_async_remote_copy(
             src_ref=src, dst_ref=dst, send_sem=send, recv_sem=recv, device_id={"ep": to}, device_id_type=MESH
         )
 
+    def gather_start(self, buf, send, recv):
+        me = self.me
+        for to in [self.at(d * (1 - 2 * self.core), 1) for d in OWN] + [self.partner()]:
+            self.copy(buf.at[me], buf.at[me], send, recv.at[me], to).start()
+
     def gather(self, buf, send, recv, landed):
         core, me = self.core, self.me
 
@@ -68,39 +77,33 @@
         def turned(d, side):
             return d if side == 0 else -d
 
-        for d in OWN:
-            pass_on(me, self.at(d * (1 - 2 * core), 1))
-        pass_on(me, self.partner())
-        landed(me)
         steps = RELAYS + tuple((d, ()) for d in LEAVES)
+        arrive(self.partner())
+        landed(me, self.partner())
 
         @pl.when(core == 1)
         def _():
             passed = 0
             for d, onward in steps:
-                for side in range(2):
-                    block = self.at(-turned(d, side), side)
+                blocks = [self.at(-turned(d, side), side) for side in range(2)]
+                for side, block in enumerate(blocks):
                     arrive(block)
                     for step in onward:
                         pass_on(block, self.at(turned(step, side), 1))
                     pass_on(block, self.partner())
                     passed += len(onward) + 1
-                    landed(block)
-            arrive(self.partner())
-            landed(self.partner())
+                landed(*blocks)
             sent(len(OWN) + 1)
             for start in range(0, passed, self.ep):
                 sent(min(self.ep, passed - start))
 
         @pl.when(core == 0)
         def _():
-            arrive(self.partner())
-            landed(self.partner())
             for d, _ in steps:
-                for side in range(2):
-                    block = self.at(-turned(d, side), side)
+                blocks = [self.at(-turned(d, side), side) for side in range(2)]
+                for block in blocks:
                     arrive(block)
-                    landed(block)
+                landed(*blocks)
             sent(len(OWN) + 1)
 
     def exchange(self, out, back, send, recv):
@@ -170,8 +173,8 @@
     ) = locals_
     out_ref, state, new_x, new_bc = outputs
     (
-        buf, buf2, buf3, stage, lhs, xraw, flat, out, back, tokf, convx, convbc,
-        stepbc, decaybc, skipbc, bcs, ybuf, xbuf, rowx, rowbc, sq, act, wide, half_out, half_in, mine, total,
+        buf, buf2, buf3, stage, narrowed, gacc, xraw, flat, out, back, tokf, convx, convbc,
+        stepbc, decaybc, skipbc, bcs, ybuf, xbuf, rowx, rowbc, sq, act, wide, half_out, half_in, total,
         send_rows, got_rows,
         wload, send1, recv1, send2, recv2, send3, recv3, hsend, hrecv, xsend, xrecv, csend, crecv,
     ) = refs
@@ -225,12 +228,17 @@
     sq[...] = jnp.zeros((64, LANES), F32)
     ready()
 
-    def landed(block):
-        both = buf[block].astype(F32)
-        for r in range(2):
-            stage[pl.ds(pl.multiple_of((block * 2 + r) * PITCH, 8), 32), :] = both[r]
-
-    comm.gather(buf, send1, recv1, landed)
+    def staged(source):
+        def landed(*blocks):
+            for block in blocks:
+                both = source[block].astype(F32)
+                for r in range(2):
+                    stage[pl.ds(pl.multiple_of((block * 2 + r) * PITCH, 8), 32), :] = both[r]
+
+        return landed
+
+    comm.gather_start(buf, send1, recv1)
+    comm.gather(buf, send1, recv1, staged(buf))
     for p in pulls[:4]:
         p.wait()
     square = jnp.zeros((64, LANES), F32)
@@ -265,11 +273,25 @@
         step = jax.nn.softplus(mine8[r * 4 : r * 4 + 1, :] + bias)
         stepbc[pl.ds(r * LANES, LANES), :] = column(step)
         decaybc[pl.ds(r * LANES, LANES), :] = column(jnp.exp(-step * rate))
+    low = lax.broadcasted_iota(jnp.int32, (32, LANES), 1) < 64
+
+    def spread_heads(source, base):
+        return jnp.where(
+            low, source[pl.ds(base, 32, stride=2), :], source[pl.ds(base + 1, 32, stride=2), :]
+        )
+
+    gacc[...] = jnp.zeros((64, 1024), F32)
+    pulls[4].wait()
+
+    def narrow(i, carry):
+        r, g = lax.div(i, 4), lax.rem(i, 4)
+        heads = state[r, pl.ds(g * 16, 16)].reshape(1024, LANES)
+        narrowed[pl.ds(pl.multiple_of(i * 1024, 1024), 1024), :] = heads.astype(BF16)
+        return carry
+
+    lax.fori_loop(0, 8, narrow, 0)
     comm.exchanged(out, back, xsend, xrecv, lambda frm: None)
     flat[...] = back[...].astype(F32).reshape(256, LANES)
-    pulls[4].wait()
-
-    low = lax.broadcasted_iota(jnp.int32, (32, LANES), 1) < 64
     for r in range(2):
         x_pre = flat[pl.ds(4 * r + 1, 32, stride=8), :]
         bc_pre = flat[pl.ds(4 * r + 2, 8, stride=32), :]
@@ -278,21 +300,32 @@
         xbuf[pl.ds(r * 32, 32), :] = x_pre
         bcs[pl.ds(16 + r * 8, 8), :] = bc_pre
         xc = jax.nn.silu(convx[pl.ds(r * 32, 32), :] + convx[pl.ds(64, 32), :] * x_pre)
-        bcs[pl.ds(r * 8, 8), :] = jax.nn.silu(convbc[pl.ds(r * 8, 8), :] + convbc[pl.ds(16, 8), :] * bc_pre)
-        per = jnp.where(
-            low,
-            stepbc[pl.ds(r * LANES, 32, stride=2), :],
-            stepbc[pl.ds(r * LANES + 1, 32, stride=2), :],
-        )
-        skip = jnp.where(low, skipbc[pl.ds(0, 32, stride=2), :], skipbc[pl.ds(1, 32, stride=2), :])
-        total[pl.ds(r * 32, 32), :] = per * xc
-        total[pl.ds(64 + r * 32, 32), :] = skip * xc
+        maps = jax.nn.silu(convbc[pl.ds(r * 8, 8), :] + convbc[pl.ds(16, 8), :] * bc_pre)
+        bcs[pl.ds(r * 8, 8), :] = maps
+        fed = spread_heads(stepbc, r * LANES) * xc
+        total[pl.ds(r * 32, 32), :] = fed
+        both = jnp.sum(maps[0:4, :] * maps[4:8, :], axis=1, keepdims=True)
+        for g in range(4):
+            i = r * 4 + g
+            y = lax.dot_general(
+                jnp.broadcast_to(maps[4 + g : 5 + g, :], (8, LANES)).astype(BF16),
+                narrowed[i * 1024 : (i + 1) * 1024, :],
+                (((1,), (1,)), ((), ())),
+                preferred_element_type=F32,
+            )
+            for k in range(8):
+                ybuf[i * 8 + k : i * 8 + k + 1, :] = y[0:1, k * LANES : (k + 1) * LANES]
+        boths = jnp.concatenate([jnp.broadcast_to(both[g : g + 1, :], (8, LANES)) for g in range(4)], axis=0)
+        gated = spread_heads(decaybc, r * LANES) * ybuf[pl.ds(r * 32, 32), :] + fed * boths
+        gated = gated + spread_heads(skipbc, 0) * xc
+        gated = gated * jax.nn.silu(flat[pl.ds(4 * r, 32, stride=8), :])
+        mean = jnp.sum(jnp.sum(gated * gated, axis=1, keepdims=True), axis=0, keepdims=True) / 4096.0
+        buf2[me, r] = (gated * lax.rsqrt(mean + 1e-6) * inner_gain[...]).astype(BF16)
 
     def group(i, carry):
         r, g = lax.div(i, 4), lax.rem(i, 4)
         cols = jnp.transpose(total[pl.ds(pl.multiple_of(i * 8, 8), 8), :])
         into = jnp.broadcast_to(bcs[pl.ds(r * 8 + g, 1), :], (LANES, LANES))
-        outof = jnp.broadcast_to(bcs[pl.ds(r * 8 + 4 + g, 1), :], (8, LANES)).astype(BF16)
         for k in range(8):
             h = g * 16 + 2 * k
             dec = jnp.concatenate(
@@ -305,26 +338,11 @@
             new = dec * state[r, pl.ds(h, 2)].reshape(LANES, LANES)
             new = new + jnp.broadcast_to(cols[:, k : k + 1], (LANES, LANES)) * into
             state[r, pl.ds(h, 2)] = new.reshape(2, 64, LANES)
-            y = lax.dot_general(
-                outof, new.astype(BF16), (((1,), (1,)), ((), ())), preferred_element_type=F32
-            )
-            ybuf[pl.ds(i * 8 + k, 1), :] = y[0:1, :]
         return carry
 
-    lax.fori_loop(0, 8, group, 0)
-    for r in range(2):
-        at = pl.ds(r * 32, 32)
-        gated = ybuf[at, :] + total[pl.ds(64 + r * 32, 32), :]
-        gated = gated * jax.nn.silu(flat[pl.ds(4 * r, 32, stride=8), :])
-        mean = jnp.sum(jnp.sum(gated * gated, axis=1, keepdims=True), axis=0, keepdims=True) / 4096.0
-        buf2[me, r] = (gated * lax.rsqrt(mean + 1e-6) * inner_gain[...]).astype(BF16)
-
-    def landed2(block):
-        both = buf2[block].astype(F32)
-        for r in range(2):
-            stage[pl.ds(pl.multiple_of((block * 2 + r) * PITCH, 8), 32), :] = both[r]
-
-    comm.gather(buf2, send2, recv2, landed2)
+    comm.gather_start(buf2, send2, recv2)
+    lax.fori_loop(0, 4, group, 0)
+    comm.gather(buf2, send2, recv2, staged(buf2))
     pulls[5].wait()
     cols_out = jnp.zeros((64, LANES), F32)
     for k in range(16):
@@ -333,20 +351,30 @@
         cols_out = cols_out + jnp.dot(part, wo[k * 256 : (k + 1) * 256, :], preferred_element_type=F32)
     buf3[me] = cols_out.astype(BF16)
 
-    def landed3(block):
-        cols = pl.ds(pl.multiple_of(block * LANES, LANES), LANES)
-        resid = (xraw[:, cols].astype(F32) + buf3[block].astype(F32)).astype(BF16).astype(F32)
-        sq[...] = sq[...] + resid * resid
-        stage[pl.ds(block, 64, stride=PITCH), :] = resid
-        lhs[:, cols] = (resid * ffn_gain[pl.ds(block, 1), :]).astype(BF16)
-
+    def landed3(*blocks):
+        part, gates, ups = [], [], []
+        for block in blocks:
+            cols = pl.ds(pl.multiple_of(block * LANES, LANES), LANES)
+            resid = (xraw[:, cols].astype(F32) + buf3[block].astype(F32)).astype(BF16).astype(F32)
+            sq[...] = sq[...] + resid * resid
+            stage[pl.ds(block, 64, stride=PITCH), :] = resid
+            part.append((resid * ffn_gain[pl.ds(block, 1), :]).astype(BF16))
+            gates.append(wg[cols, :])
+            ups.append(wu[cols, :])
+        part = jnp.concatenate(part, axis=1)
+        for at, w in ((0, gates), (512, ups)):
+            at = pl.ds(at, 512)
+            gacc[:, at] = gacc[:, at] + jnp.dot(
+                part, jnp.concatenate(w, axis=0), preferred_element_type=F32
+            )
+
+    comm.gather_start(buf3, send3, recv3)
+    lax.fori_loop(4, 8, group, 0)
+    pulls[6].wait()
+    pulls[7].wait()
     comm.gather(buf3, send3, recv3, landed3)
     scale = lax.rsqrt(jnp.sum(sq[...], axis=1, keepdims=True) / 4096.0 + 1e-6)
-    pulls[6].wait()
-    pulls[7].wait()
-    left = lhs[...]
-    gate = jnp.dot(left, wg[...], preferred_element_type=F32) * scale
-    up = jnp.dot(left, wu[...], preferred_element_type=F32) * scale
+    gate, up = gacc[:, 0:512] * scale, gacc[:, 512:1024] * scale
     act[...] = (jax.nn.silu(gate) * up).astype(BF16)
     pulls[8].wait()
     lanes32 = lax.broadcasted_iota(jnp.int32, (32, LANES), 1)
@@ -356,29 +384,36 @@
         wide[pl.ds(r, 32, stride=2), :] = jnp.broadcast_to(picked, (32, LANES))
     weight = jnp.concatenate([wide[...]] * 4, axis=1)
 
-    def expert(half, k):
-        cols = pl.ds(pl.multiple_of(half * 2048 + k * 512, 512), 512)
-        y = jnp.dot(act[...], wd[:, cols], preferred_element_type=F32).astype(BF16).astype(F32)
+    def expert(half, part):
+        at = pl.ds(pl.multiple_of(half * 2048 + part * 512, 512), 512)
+        y = jnp.dot(act[...], wd[:, at], preferred_element_type=F32).astype(BF16).astype(F32)
         return y * weight
 
-    for k in range(4):
-        half_out[:, k * 512 : (k + 1) * 512] = expert(1 - core, k).astype(BF16)
-    swap = comm.copy(half_out, half_in, hsend, hrecv, comm.partner())
-    swap.start()
-    for k in range(4):
-        mine[:, k * 512 : (k + 1) * 512] = expert(core, k)
-    swap.wait()
-    for j in range(16):
-        cols = slice(j * LANES, (j + 1) * LANES)
-        total[pl.ds(j, 64, stride=24), :] = mine[:, cols] + half_in[:, cols].astype(F32)
-
-    def pack(t, carry):
-        for r in range(2):
-            send_rows[t, r] = total[pl.ds(pl.multiple_of((t * 2 + r) * 24, 8), 16), :].astype(BF16)
-        return carry
-
-    lax.fori_loop(0, ep, pack, 0)
-    comm.exchange(send_rows, got_rows, csend, crecv)
+    swaps = []
+    for ch in range(2):
+        for k in range(2):
+            half_out[ch, :, k * 512 : (k + 1) * 512] = expert(1 - core, 2 * ch + k).astype(BF16)
+        swaps.append(
+            comm.copy(half_out.at[ch], half_in.at[ch], hsend.at[ch], hrecv.at[ch], comm.partner())
+        )
+        swaps[ch].start()
+    for ch in range(2):
+        own = [expert(core, 2 * ch + k) for k in range(2)]
+        swaps[ch].wait()
+        for j in range(8):
+            k, cols = j // 4, slice(j % 4 * LANES, (j % 4 + 1) * LANES)
+            total[pl.ds(8 * ch + j, 64, stride=24), :] = own[k][:, cols] + half_in[
+                ch, :, j * LANES : (j + 1) * LANES
+            ].astype(F32)
+
+        def pack(t, carry, ch=ch):
+            for r in range(2):
+                at = pl.ds(pl.multiple_of((t * 2 + r) * 24 + 8 * ch, 8), 8)
+                send_rows[ch, t, r] = total[at, :].astype(BF16)
+            return carry
+
+        lax.fori_loop(0, ep, pack, 0)
+        comm.exchange(send_rows.at[ch], got_rows.at[ch], csend.at[ch], crecv.at[ch])
     for r in range(2):
         tokf[pl.ds(r * 32, 32), :] = stage[pl.ds(pl.multiple_of((me * 2 + r) * PITCH, 8), 32), :]
     for r in range(2):
@@ -389,13 +424,15 @@
         new[1] = old[2]
         new[2] = row[...].astype(BF16)
 
-    def arrived(frm):
-        h = lax.rem(frm, 2)
-        for r in range(2):
-            at = pl.ds(pl.multiple_of(r * 32 + h * 16, 8), 16)
-            tokf[at, :] = tokf[at, :] + got_rows[frm, r].astype(F32)
-
-    comm.exchanged(send_rows, got_rows, csend, crecv, arrived)
+    for ch in range(2):
+
+        def arrived(frm, ch=ch):
+            h = lax.rem(frm, 2)
+            for r in range(2):
+                at = pl.ds(pl.multiple_of(r * 32 + h * 16 + ch * 8, 8), 8)
+                tokf[at, :] = tokf[at, :] + got_rows[ch, frm, r].astype(F32)
+
+        comm.exchanged(send_rows.at[ch], got_rows.at[ch], csend.at[ch], crecv.at[ch], arrived)
     for r in range(2):
         row_of(rowx, r, tokf, r * 32, 32)
     out_ref[...] = rowx[...].astype(BF16)
@@ -423,16 +460,16 @@
         scratch_shapes=[
             *local,
             v((ep, 2, 32, LANES), BF16), v((ep, 2, 32, LANES), BF16), v((ep, 64, LANES), BF16),
-            v((64 * PITCH, LANES), F32), v((64, 4096), BF16), v((64, 4096), BF16),
+            v((64 * PITCH, LANES), F32), v((8192, LANES), BF16), v((64, 1024), F32), v((64, 4096), BF16),
             v((256, LANES), F32), v((ep, 8, LANES), BF16), v((ep, 8, LANES), BF16), v((64, LANES), F32),
             v((96, LANES), F32), v((24, LANES), F32),
             v((256, LANES), F32), v((256, LANES), F32), v((LANES, LANES), F32), v((32, LANES), F32),
             v((64, LANES), F32), v((64, LANES), F32), v((2, 4096), F32), v((2, 1024), F32), v((64, LANES), F32),
-            v((64, 512), BF16), v((64, LANES), F32), v((64, 2048), BF16), v((64, 2048), BF16),
-            v((64, 2048), F32), v((64 * 24, LANES), F32),
-            v((ep, 2, 16, LANES), BF16), v((ep, 2, 16, LANES), BF16),
-            dma((22,)), dma, dma((ep,)), dma, dma((ep,)), dma, dma((ep,)), dma, dma, dma, dma((ep,)),
-            dma, dma((ep,)),
+            v((64, 512), BF16), v((64, LANES), F32), v((2, 64, 1024), BF16), v((2, 64, 1024), BF16),
+            v((64 * 24, LANES), F32),
+            v((2, ep, 2, 8, LANES), BF16), v((2, ep, 2, 8, LANES), BF16),
+            dma((22,)), dma, dma((ep,)), dma, dma((ep,)), dma, dma((ep,)), dma((2,)), dma((2,)), dma, dma((ep,)),
+            dma((2,)), dma((2, ep)),
         ],
         compiler_params=pltpu.CompilerParams(
             collective_id=0, has_side_effects=True, vmem_limit_bytes=VMEM_LIMIT

time: 86.8 us -> 80.9 us (0.932)
  Pallas kernels: 86 us -> 80.1 us
    pallas_call x1, Pallas kernels: 83.9 us -> 78 us  [layer(): pl.pallas_call(functools.partial(layer_kernel, ep, len(args), len(outs)),...]
where the time goes in v4:
time: 80.9 us; the launch traced here: 80.7 us
  Pallas kernels  80.1 us (99%)
    pallas_call x1, Pallas kernels, layer(): pl.pallas_call(functools.partial(layer_kernel, ep, len(args), len(outs)),...  78 us
    pallas_call x1, Pallas kernels, layer(): pl.pallas_call(flush_kernel, out_shape=outs, in_specs=[vmem()] * len(outs...  2.06 us

profile of v4, /device:TPU:69, one launch (start us, length us, event | category | flops | bytes accessed | tf_op | source)
XLA Modules:
  0.0 80.7 jit_solution(17425626676679434490)
XLA Ops:
  0.6 78.0 %layer.1 = (bf16[2,4096]{1,0:T(2,128)(2,1)S(1)}, f32[2,64,64,128]{3,2,1,0:T(8,128)S(1)}, bf16[3,2,4096]{2,1,0:T(2,128)(2,1)S(1)}, bf16[3,2,1024]{2,1,0:T(2,128)(2,1)S(1)}) custom-call(bf16[2,4096]{1,0:T(2,128)(2,1)} %refs_0_.1, f32[32,128]{1,0:T(8,128)} %bitcast.15, bf16[4096,128]{1,0:T(8,128)(2,1)} %refs_2_.1, bf16[4096,128]{1,0:T(8,128)(2,1)} %refs_3_.1, ...), custom_call_target="tpu_custom_call" | custom-call | tf_op jit(solution)/shard_map/layer/pallas_call | solution.py:455
  78.7 2.1 %flush.1 = (bf16[2,4096]{1,0:T(2,128)(2,1)}, f32[2,64,64,128]{3,2,1,0:T(8,128)}, bf16[3,2,4096]{2,1,0:T(2,128)(2,1)}, bf16[3,2,1024]{2,1,0:T(2,128)(2,1)}) custom-call(bf16[2,4096]{1,0:T(2,128)(2,1)S(1)} %get-tuple-element.12.refs_0_, f32[2,64,64,128]{3,2,1,0:T(8,128)S(1)} %get-tuple-element.13.refs_1_, bf16[3,2,4096]{2,1,0:T(2,128)(2,1)S(1)} %get-tuple-element.14.refs_2_, ...), custom_call_target="tpu_custom_call" | custom-call | tf_op jit(solution)/shard_map/flush/pallas_call | solution.py:479

commit v5 on v4

--- a/solution.py
+++ b/solution.py
@@ -19,7 +19,11 @@
 OWN = (6, -6, 3, -3, 1, -1)
 RELAYS = ((3, (1, -1)), (-3, (1, -1)), (6, (2, 1, -1)), (-6, (1, -1)))
 GREET = (1, -1, 2, -2, 3, -3, 6, -6)
-LEAVES = (1, -1, 2, -2, 4, -4, 5, -5, 7, -7, 8)
+GROUPS = ((3, -3), (6, -6, 1, -1), (2, -2, 4, -4), (5, -5, 7, -7, 8))
+
+
+def turned(d, side):
+    return d if side == 0 else -d
 
 
 class Comm:
@@ -74,37 +78,86 @@
             whole = buf.at[pl.ds(0, n)]
             self.copy(whole, whole, send, recv.at[0], me).wait_send()
 
-        def turned(d, side):
-            return d if side == 0 else -d
-
-        steps = RELAYS + tuple((d, ()) for d in LEAVES)
-        arrive(self.partner())
-        landed(me, self.partner())
+        relays = dict(RELAYS)
 
         @pl.when(core == 1)
         def _():
-            passed = 0
-            for d, onward in steps:
-                blocks = [self.at(-turned(d, side), side) for side in range(2)]
-                for side, block in enumerate(blocks):
-                    arrive(block)
-                    for step in onward:
-                        pass_on(block, self.at(turned(step, side), 1))
-                    pass_on(block, self.partner())
-                    passed += len(onward) + 1
-                landed(*blocks)
+            arrive(self.partner())
+            blocks, passed = [me, self.partner()], 0
+            for offsets in GROUPS:
+                for d in offsets:
+                    for side in range(2):
+                        block = self.at(-turned(d, side), side)
+                        arrive(block)
+                        for step in relays.get(d, ()):
+                            pass_on(block, self.at(turned(step, side), 1))
+                            passed += 1
+                        pass_on(block, self.partner())
+                        passed += 1
+                        blocks.append(block)
+                landed(blocks)
+                blocks = []
             sent(len(OWN) + 1)
             for start in range(0, passed, self.ep):
                 sent(min(self.ep, passed - start))
 
         @pl.when(core == 0)
         def _():
-            for d, _ in steps:
-                blocks = [self.at(-turned(d, side), side) for side in range(2)]
-                for block in blocks:
-                    arrive(block)
-                landed(*blocks)
+            arrive(self.partner())
+            blocks = [me, self.partner()]
+            for offsets in GROUPS:
+                for d in offsets:
+                    for side in range(2):
+                        block = self.at(-turned(d, side), side)
+                        arrive(block)
+                        blocks.append(block)
+                landed(blocks)
+                blocks = []
             sent(len(OWN) + 1)
+
+    def reduce(self, own, parts, relay_in, relay_out, final_in, sums, send, relay_sem, final_sem):
+        core, me = self.core, self.me
+        slots = {(d, step): i for i, (d, step) in enumerate((d, step) for d, on in RELAYS for step in on)}
+        finals = {d: i for i, d in enumerate(OWN)}
+        relays = [d for d, _ in RELAYS]
+        per = len(slots)
+
+        def leaf(d, step, side):
+            slot = side * per + slots[d, step]
+            to = self.at(-turned(step, side), core)
+            part = parts.at[self.at(-turned(d + step, side), side)]
+            return self.copy(part, relay_in.at[slot], send, relay_sem.at[slot], to)
+
+        def final(d, side, source):
+            slot = side * len(OWN) + finals[d]
+            return self.copy(source, final_in.at[slot], send, final_sem.at[slot], self.at(-turned(d, side), core))
+
+        for d, onward in reversed(RELAYS):
+            for step in onward:
+                for side in range(2):
+                    leaf(d, step, side).start()
+        for d in OWN:
+            if d not in relays:
+                for side in range(2):
+                    final(d, side, parts.at[self.at(-turned(d, side), side)]).start()
+        for d, onward in reversed(RELAYS):
+            for side in range(2):
+                total = own(self.at(-turned(d, side), side))
+                for step in onward:
+                    slot = side * per + slots[d, step]
+                    leaf(d, step, side).wait_recv()
+                    total = total + relay_in[slot].astype(F32)
+                at = side * len(relays) + relays.index(d)
+                relay_out[at] = total.astype(BF16)
+                final(d, side, relay_out.at[at]).start()
+        for side in range(2):
+            sums[side] = own(self.z * 2 + side)
+        for d in reversed(OWN):
+            for side in range(2):
+                final(d, side, relay_out.at[0]).wait_recv()
+                sums[side] = sums[side] + final_in[side * len(OWN) + finals[d]].astype(F32)
+        whole = parts.at[pl.ds(0, 2 * (per + len(OWN)))]
+        self.copy(whole, whole, send, final_sem.at[0], me).wait_send()
 
     def exchange(self, out, back, send, recv):
         me, ep, nz = self.me, self.ep, self.nz
@@ -175,8 +228,8 @@
     (
         buf, buf2, buf3, stage, narrowed, gacc, xraw, flat, out, back, tokf, convx, convbc,
         stepbc, decaybc, skipbc, bcs, ybuf, xbuf, rowx, rowbc, sq, act, wide, half_out, half_in, total,
-        send_rows, got_rows,
-        wload, send1, recv1, send2, recv2, send3, recv3, hsend, hrecv, xsend, xrecv, csend, crecv,
+        send_rows, relay_in, relay_out, final_in, sums, handed,
+        wload, send1, recv1, send2, recv2, send3, recv3, hsend, hrecv, xsend, xrecv, csend, relay_sem, final_sem, fsend, frecv,
     ) = refs
     comm = Comm(ep)
     me, core = comm.me, comm.core
@@ -202,6 +255,8 @@
     for r in range(2):
         rows_of(tokf, rows[r : r + 1, :], r * 32)
     buf[me] = tall(tokf[...], 2).astype(BF16)
+    ready()
+    comm.gather_start(buf, send1, recv1)
     for p in early[1:]:
         p.wait()
     for conv, taps, dst, n in ((conv_x, conv_x_w, convx, 32), (conv_bc, conv_bc_w, convbc, 8)):
@@ -226,10 +281,9 @@
 
     skipbc[...] = column(jnp.concatenate([skip_gain[...], blank], axis=1))
     sq[...] = jnp.zeros((64, LANES), F32)
-    ready()
 
     def staged(source):
-        def landed(*blocks):
+        def landed(blocks):
             for block in blocks:
                 both = source[block].astype(F32)
                 for r in range(2):
@@ -237,7 +291,6 @@
 
         return landed
 
-    comm.gather_start(buf, send1, recv1)
     comm.gather(buf, send1, recv1, staged(buf))
     for p in pulls[:4]:
         p.wait()
@@ -351,22 +404,22 @@
         cols_out = cols_out + jnp.dot(part, wo[k * 256 : (k + 1) * 256, :], preferred_element_type=F32)
     buf3[me] = cols_out.astype(BF16)
 
-    def landed3(*blocks):
-        part, gates, ups = [], [], []
-        for block in blocks:
-            cols = pl.ds(pl.multiple_of(block * LANES, LANES), LANES)
-            resid = (xraw[:, cols].astype(F32) + buf3[block].astype(F32)).astype(BF16).astype(F32)
-            sq[...] = sq[...] + resid * resid
-            stage[pl.ds(block, 64, stride=PITCH), :] = resid
-            part.append((resid * ffn_gain[pl.ds(block, 1), :]).astype(BF16))
-            gates.append(wg[cols, :])
-            ups.append(wu[cols, :])
-        part = jnp.concatenate(part, axis=1)
-        for at, w in ((0, gates), (512, ups)):
-            at = pl.ds(at, 512)
-            gacc[:, at] = gacc[:, at] + jnp.dot(
-                part, jnp.concatenate(w, axis=0), preferred_element_type=F32
-            )
+    def landed3(blocks):
+        gates, ups, square = gacc[:, 0:512], gacc[:, 512:1024], sq[...]
+        for pair in zip(blocks[::2], blocks[1::2], strict=True):
+            part, gate_rows, up_rows = [], [], []
+            for block in pair:
+                cols = pl.ds(pl.multiple_of(block * LANES, LANES), LANES)
+                resid = (xraw[:, cols].astype(F32) + buf3[block].astype(F32)).astype(BF16).astype(F32)
+                square = square + resid * resid
+                stage[pl.ds(block, 64, stride=PITCH), :] = resid
+                part.append((resid * ffn_gain[pl.ds(block, 1), :]).astype(BF16))
+                gate_rows.append(wg[cols, :])
+                up_rows.append(wu[cols, :])
+            part = jnp.concatenate(part, axis=1)
+            gates = gates + jnp.dot(part, jnp.concatenate(gate_rows, axis=0), preferred_element_type=F32)
+            ups = ups + jnp.dot(part, jnp.concatenate(up_rows, axis=0), preferred_element_type=F32)
+        gacc[:, 0:512], gacc[:, 512:1024], sq[...] = gates, ups, square
 
     comm.gather_start(buf3, send3, recv3)
     lax.fori_loop(4, 8, group, 0)
@@ -406,14 +459,21 @@
                 ch, :, j * LANES : (j + 1) * LANES
             ].astype(F32)
 
-        def pack(t, carry, ch=ch):
-            for r in range(2):
-                at = pl.ds(pl.multiple_of((t * 2 + r) * 24 + 8 * ch, 8), 8)
-                send_rows[ch, t, r] = total[at, :].astype(BF16)
-            return carry
-
-        lax.fori_loop(0, ep, pack, 0)
-        comm.exchange(send_rows.at[ch], got_rows.at[ch], csend.at[ch], crecv.at[ch])
+
+    def pack(t, carry):
+        for r in range(2):
+            send_rows[t, r] = total[pl.ds(pl.multiple_of((t * 2 + r) * 24, 8), 16), :].astype(BF16)
+        return carry
+
+    lax.fori_loop(0, ep, pack, 0)
+
+    def chip_rows(device):
+        at = [pl.ds(pl.multiple_of((device * 2 + r) * 24, 8), 16) for r in range(2)]
+        return jnp.stack([total[a, :] for a in at])
+
+    comm.reduce(chip_rows, send_rows, relay_in, relay_out, final_in, sums, csend, relay_sem, final_sem)
+    hand = comm.copy(sums.at[1 - core], handed, fsend, frecv, comm.partner())
+    hand.start()
     for r in range(2):
         tokf[pl.ds(r * 32, 32), :] = stage[pl.ds(pl.multiple_of((me * 2 + r) * PITCH, 8), 32), :]
     for r in range(2):
@@ -424,15 +484,11 @@
         new[1] = old[2]
         new[2] = row[...].astype(BF16)
 
-    for ch in range(2):
-
-        def arrived(frm, ch=ch):
-            h = lax.rem(frm, 2)
-            for r in range(2):
-                at = pl.ds(pl.multiple_of(r * 32 + h * 16 + ch * 8, 8), 8)
-                tokf[at, :] = tokf[at, :] + got_rows[ch, frm, r].astype(F32)
-
-        comm.exchanged(send_rows.at[ch], got_rows.at[ch], csend.at[ch], crecv.at[ch], arrived)
+    hand.wait()
+    for half, source in ((core, sums.at[core]), (1 - core, handed)):
+        for r in range(2):
+            at = pl.ds(pl.multiple_of(r * 32 + half * 16, 8), 16)
+            tokf[at, :] = tokf[at, :] + source[r]
     for r in range(2):
         row_of(rowx, r, tokf, r * 32, 32)
     out_ref[...] = rowx[...].astype(BF16)
@@ -467,9 +523,10 @@
             v((64, LANES), F32), v((64, LANES), F32), v((2, 4096), F32), v((2, 1024), F32), v((64, LANES), F32),
             v((64, 512), BF16), v((64, LANES), F32), v((2, 64, 1024), BF16), v((2, 64, 1024), BF16),
             v((64 * 24, LANES), F32),
-            v((2, ep, 2, 8, LANES), BF16), v((2, ep, 2, 8, LANES), BF16),
+            v((ep, 2, 16, LANES), BF16), v((18, 2, 16, LANES), BF16), v((8, 2, 16, LANES), BF16),
+            v((12, 2, 16, LANES), BF16), v((2, 2, 16, LANES), F32), v((2, 16, LANES), F32),
             dma((22,)), dma, dma((ep,)), dma, dma((ep,)), dma, dma((ep,)), dma((2,)), dma((2,)), dma, dma((ep,)),
-            dma((2,)), dma((2, ep)),
+            dma, dma((18,)), dma((12,)), dma, dma,
         ],
         compiler_params=pltpu.CompilerParams(
             collective_id=0, has_side_effects=True, vmem_limit_bytes=VMEM_LIMIT

time: 80.9 us -> 77.7 us (0.960)
  Pallas kernels: 80.1 us -> 76.9 us
    pallas_call x1, Pallas kernels: 78 us -> 74.8 us  [layer(): pl.pallas_call(functools.partial(layer_kernel, ep, len(args), len(outs)),...]
where the time goes in v5:
time: 77.7 us; the launch traced here: 77.5 us
  Pallas kernels  76.9 us (99%)
    pallas_call x1, Pallas kernels, layer(): pl.pallas_call(functools.partial(layer_kernel, ep, len(args), len(outs)),...  74.8 us
    pallas_call x1, Pallas kernels, layer(): pl.pallas_call(flush_kernel, out_shape=outs, in_specs=[vmem()] * len(outs...  2.06 us

profile of v5, /device:TPU:69, one launch (start us, length us, event | category | flops | bytes accessed | tf_op | source)
XLA Modules:
  0.0 77.5 jit_solution(539369471746541760)
XLA Ops:
  0.6 74.8 %layer.1 = (bf16[2,4096]{1,0:T(2,128)(2,1)S(1)}, f32[2,64,64,128]{3,2,1,0:T(8,128)S(1)}, bf16[3,2,4096]{2,1,0:T(2,128)(2,1)S(1)}, bf16[3,2,1024]{2,1,0:T(2,128)(2,1)S(1)}) custom-call(bf16[2,4096]{1,0:T(2,128)(2,1)} %refs_0_.1, f32[32,128]{1,0:T(8,128)} %bitcast.15, bf16[4096,128]{1,0:T(8,128)(2,1)} %refs_2_.1, bf16[4096,128]{1,0:T(8,128)(2,1)} %refs_3_.1, ...), custom_call_target="tpu_custom_call" | custom-call | tf_op jit(solution)/shard_map/layer/pallas_call | solution.py:511
  75.5 2.1 %flush.1 = (bf16[2,4096]{1,0:T(2,128)(2,1)}, f32[2,64,64,128]{3,2,1,0:T(8,128)}, bf16[3,2,4096]{2,1,0:T(2,128)(2,1)}, bf16[3,2,1024]{2,1,0:T(2,128)(2,1)}) custom-call(bf16[2,4096]{1,0:T(2,128)(2,1)S(1)} %get-tuple-element.12.refs_0_, f32[2,64,64,128]{3,2,1,0:T(8,128)S(1)} %get-tuple-element.13.refs_1_, bf16[3,2,4096]{2,1,0:T(2,128)(2,1)S(1)} %get-tuple-element.14.refs_2_, ...), custom_call_target="tpu_custom_call" | custom-call | tf_op jit(solution)/shard_map/flush/pallas_call | solution.py:536

commit v6 on v5

--- a/solution.py
+++ b/solution.py
@@ -18,8 +18,10 @@
 
 OWN = (6, -6, 3, -3, 1, -1)
 RELAYS = ((3, (1, -1)), (-3, (1, -1)), (6, (2, 1, -1)), (-6, (1, -1)))
-GREET = (1, -1, 2, -2, 3, -3, 6, -6)
-GROUPS = ((3, -3), (6, -6, 1, -1), (2, -2, 4, -4), (5, -5, 7, -7, 8))
+OWN_FIRST = (3, -3, 1, -1)
+RELAYS_FIRST = ((3, (3, 1, -1)), (-3, (-3, 1, -1)), (6, (2, 1, -1)), (-6, (1, -1)))
+GREET = (1, -1, 2, -2, 3, -3)
+GROUPS = ((3, -3), (6, -6, 1, -1), (2, -2, 4, -4, 5, -5), (7, -7, 8))
 
 
 def turned(d, side):
@@ -60,12 +62,12 @@
             src_ref=src, dst_ref=dst, send_sem=send, recv_sem=recv, device_id={"ep": to}, device_id_type=MESH
         )
 
-    def gather_start(self, buf, send, recv):
+    def gather_start(self, buf, send, recv, own=OWN):
         me = self.me
-        for to in [self.at(d * (1 - 2 * self.core), 1) for d in OWN] + [self.partner()]:
+        for to in [self.at(d * (1 - 2 * self.core), 1) for d in own] + [self.partner()]:
             self.copy(buf.at[me], buf.at[me], send, recv.at[me], to).start()
 
-    def gather(self, buf, send, recv, landed):
+    def gather(self, buf, send, recv, landed, own=OWN, onward=RELAYS):
         core, me = self.core, self.me
 
         def pass_on(block, to):
@@ -78,7 +80,7 @@
             whole = buf.at[pl.ds(0, n)]
             self.copy(whole, whole, send, recv.at[0], me).wait_send()
 
-        relays = dict(RELAYS)
+        relays = dict(onward)
 
         @pl.when(core == 1)
         def _():
@@ -95,9 +97,11 @@
                         pass_on(block, self.partner())
                         passed += 1
                         blocks.append(block)
+                if offsets == GROUPS[-2]:
+                    continue
                 landed(blocks)
                 blocks = []
-            sent(len(OWN) + 1)
+            sent(len(own) + 1)
             for start in range(0, passed, self.ep):
                 sent(min(self.ep, passed - start))
 
@@ -113,14 +117,13 @@
                         blocks.append(block)
                 landed(blocks)
                 blocks = []
-            sent(len(OWN) + 1)
+            sent(len(own) + 1)
 
     def reduce(self, own, parts, relay_in, relay_out, final_in, sums, send, relay_sem, final_sem):
         core, me = self.core, self.me
         slots = {(d, step): i for i, (d, step) in enumerate((d, step) for d, on in RELAYS for step in on)}
-        finals = {d: i for i, d in enumerate(OWN)}
         relays = [d for d, _ in RELAYS]
-        per = len(slots)
+        per, ends = len(slots), len(OWN) + 1
 
         def leaf(d, step, side):
             slot = side * per + slots[d, step]
@@ -128,35 +131,38 @@
             part = parts.at[self.at(-turned(d + step, side), side)]
             return self.copy(part, relay_in.at[slot], send, relay_sem.at[slot], to)
 
-        def final(d, side, source):
-            slot = side * len(OWN) + finals[d]
-            return self.copy(source, final_in.at[slot], send, final_sem.at[slot], self.at(-turned(d, side), core))
+        def final(i, half, source, to):
+            slot = half * ends + i
+            return self.copy(source, final_in.at[slot], send, final_sem.at[slot], to)
 
         for d, onward in reversed(RELAYS):
             for step in onward:
                 for side in range(2):
                     leaf(d, step, side).start()
-        for d in OWN:
+        for i, d in enumerate(OWN):
             if d not in relays:
                 for side in range(2):
-                    final(d, side, parts.at[self.at(-turned(d, side), side)]).start()
+                    to = self.at(-turned(d, side), side)
+                    final(i, core, parts.at[to], to).start()
+        final(ends - 1, core, parts.at[self.partner()], self.partner()).start()
         for d, onward in reversed(RELAYS):
             for side in range(2):
-                total = own(self.at(-turned(d, side), side))
+                to = self.at(-turned(d, side), side)
+                total = own(to)
                 for step in onward:
-                    slot = side * per + slots[d, step]
                     leaf(d, step, side).wait_recv()
-                    total = total + relay_in[slot].astype(F32)
+                    total = total + relay_in[side * per + slots[d, step]].astype(F32)
                 at = side * len(relays) + relays.index(d)
                 relay_out[at] = total.astype(BF16)
-                final(d, side, relay_out.at[at]).start()
-        for side in range(2):
-            sums[side] = own(self.z * 2 + side)
-        for d in reversed(OWN):
-            for side in range(2):
-                final(d, side, relay_out.at[0]).wait_recv()
-                sums[side] = sums[side] + final_in[side * len(OWN) + finals[d]].astype(F32)
-        whole = parts.at[pl.ds(0, 2 * (per + len(OWN)))]
+                final(OWN.index(d), core, relay_out.at[at], to).start()
+        final(ends - 1, 1 - core, relay_out.at[0], me).wait_recv()
+        sums[core] = own(me)
+        sums[1 - core] = final_in[(1 - core) * ends + ends - 1].astype(F32)
+        for i in reversed(range(len(OWN))):
+            for half in range(2):
+                final(i, half, relay_out.at[0], me).wait_recv()
+                sums[half] = sums[half] + final_in[half * ends + i].astype(F32)
+        whole = parts.at[pl.ds(0, 2 * (per + len(OWN)) + 1)]
         self.copy(whole, whole, send, final_sem.at[0], me).wait_send()
 
     def exchange(self, out, back, send, recv):
@@ -228,8 +234,8 @@
     (
         buf, buf2, buf3, stage, narrowed, gacc, xraw, flat, out, back, tokf, convx, convbc,
         stepbc, decaybc, skipbc, bcs, ybuf, xbuf, rowx, rowbc, sq, act, wide, half_out, half_in, total,
-        send_rows, relay_in, relay_out, final_in, sums, handed,
-        wload, send1, recv1, send2, recv2, send3, recv3, hsend, hrecv, xsend, xrecv, csend, relay_sem, final_sem, fsend, frecv,
+        send_rows, relay_in, relay_out, final_in, sums,
+        wload, send1, recv1, send2, recv2, send3, recv3, hsend, hrecv, xsend, xrecv, csend, relay_sem, final_sem,
     ) = refs
     comm = Comm(ep)
     me, core = comm.me, comm.core
@@ -256,7 +262,7 @@
         rows_of(tokf, rows[r : r + 1, :], r * 32)
     buf[me] = tall(tokf[...], 2).astype(BF16)
     ready()
-    comm.gather_start(buf, send1, recv1)
+    comm.gather_start(buf, send1, recv1, OWN_FIRST)
     for p in early[1:]:
         p.wait()
     for conv, taps, dst, n in ((conv_x, conv_x_w, convx, 32), (conv_bc, conv_bc_w, convbc, 8)):
@@ -291,7 +297,7 @@
 
         return landed
 
-    comm.gather(buf, send1, recv1, staged(buf))
+    comm.gather(buf, send1, recv1, staged(buf), OWN_FIRST, RELAYS_FIRST)
     for p in pulls[:4]:
         p.wait()
     square = jnp.zeros((64, LANES), F32)
@@ -394,6 +400,13 @@
         return carry
 
     comm.gather_start(buf2, send2, recv2)
+    for r in range(2):
+        row_of(rowx, r, xbuf, r * 32, 32)
+        row_of(rowbc, r, bcs, 16 + r * 8, 8)
+    for old, new, row in ((conv_x, new_x, rowx), (conv_bc, new_bc, rowbc)):
+        new[0] = old[1]
+        new[1] = old[2]
+        new[2] = row[...].astype(BF16)
     lax.fori_loop(0, 4, group, 0)
     comm.gather(buf2, send2, recv2, staged(buf2))
     pulls[5].wait()
@@ -471,24 +484,13 @@
         at = [pl.ds(pl.multiple_of((device * 2 + r) * 24, 8), 16) for r in range(2)]
         return jnp.stack([total[a, :] for a in at])
 
+    for r in range(2):
+        tokf[pl.ds(r * 32, 32), :] = stage[pl.ds(pl.multiple_of((me * 2 + r) * PITCH, 8), 32), :]
     comm.reduce(chip_rows, send_rows, relay_in, relay_out, final_in, sums, csend, relay_sem, final_sem)
-    hand = comm.copy(sums.at[1 - core], handed, fsend, frecv, comm.partner())
-    hand.start()
-    for r in range(2):
-        tokf[pl.ds(r * 32, 32), :] = stage[pl.ds(pl.multiple_of((me * 2 + r) * PITCH, 8), 32), :]
-    for r in range(2):
-        row_of(rowx, r, xbuf, r * 32, 32)
-        row_of(rowbc, r, bcs, 16 + r * 8, 8)
-    for old, new, row in ((conv_x, new_x, rowx), (conv_bc, new_bc, rowbc)):
-        new[0] = old[1]
-        new[1] = old[2]
-        new[2] = row[...].astype(BF16)
-
-    hand.wait()
-    for half, source in ((core, sums.at[core]), (1 - core, handed)):
+    for half in range(2):
         for r in range(2):
-            at = pl.ds(pl.multiple_of(r * 32 + half * 16, 8), 16)
-            tokf[at, :] = tokf[at, :] + source[r]
+            at = pl.ds(r * 32 + half * 16, 16)
+            tokf[at, :] = tokf[at, :] + sums[half, r]
     for r in range(2):
         row_of(rowx, r, tokf, r * 32, 32)
     out_ref[...] = rowx[...].astype(BF16)
@@ -524,9 +526,9 @@
             v((64, 512), BF16), v((64, LANES), F32), v((2, 64, 1024), BF16), v((2, 64, 1024), BF16),
             v((64 * 24, LANES), F32),
             v((ep, 2, 16, LANES), BF16), v((18, 2, 16, LANES), BF16), v((8, 2, 16, LANES), BF16),
-            v((12, 2, 16, LANES), BF16), v((2, 2, 16, LANES), F32), v((2, 16, LANES), F32),
+            v((14, 2, 16, LANES), BF16), v((2, 2, 16, LANES), F32),
             dma((22,)), dma, dma((ep,)), dma, dma((ep,)), dma, dma((ep,)), dma((2,)), dma((2,)), dma, dma((ep,)),
-            dma, dma((18,)), dma((12,)), dma, dma,
+            dma, dma((18,)), dma((14,)),
         ],
         compiler_params=pltpu.CompilerParams(
             collective_id=0, has_side_effects=True, vmem_limit_bytes=VMEM_LIMIT

time: 77.7 us -> 75.5 us (0.972)
  Pallas kernels: 76.9 us -> 74.7 us
    pallas_call x1, Pallas kernels: 74.8 us -> 72.7 us  [layer(): pl.pallas_call(functools.partial(layer_kernel, ep, len(args), len(outs)),...]
where the time goes in v6:
time: 75.5 us; the launch traced here: 75.4 us
  Pallas kernels  74.7 us (99%)
    pallas_call x1, Pallas kernels, layer(): pl.pallas_call(functools.partial(layer_kernel, ep, len(args), len(outs)),...  72.7 us
    pallas_call x1, Pallas kernels, layer(): pl.pallas_call(flush_kernel, out_shape=outs, in_specs=[vmem()] * len(outs...  2.06 us

profile of v6, /device:TPU:69, one launch (start us, length us, event | category | flops | bytes accessed | tf_op | source)
XLA Modules:
  0.0 75.4 jit_solution(12084181851057670686)
XLA Ops:
  0.6 72.7 %layer.1 = (bf16[2,4096]{1,0:T(2,128)(2,1)S(1)}, f32[2,64,64,128]{3,2,1,0:T(8,128)S(1)}, bf16[3,2,4096]{2,1,0:T(2,128)(2,1)S(1)}, bf16[3,2,1024]{2,1,0:T(2,128)(2,1)S(1)}) custom-call(bf16[2,4096]{1,0:T(2,128)(2,1)} %refs_0_.1, f32[32,128]{1,0:T(8,128)} %bitcast.15, bf16[4096,128]{1,0:T(8,128)(2,1)} %refs_2_.1, bf16[4096,128]{1,0:T(8,128)(2,1)} %refs_3_.1, ...), custom_call_target="tpu_custom_call" | custom-call | tf_op jit(solution)/shard_map/layer/pallas_call | solution.py:513
  73.3 2.1 %flush.1 = (bf16[2,4096]{1,0:T(2,128)(2,1)}, f32[2,64,64,128]{3,2,1,0:T(8,128)}, bf16[3,2,4096]{2,1,0:T(2,128)(2,1)}, bf16[3,2,1024]{2,1,0:T(2,128)(2,1)}) custom-call(bf16[2,4096]{1,0:T(2,128)(2,1)S(1)} %get-tuple-element.12.refs_0_, f32[2,64,64,128]{3,2,1,0:T(8,128)S(1)} %get-tuple-element.13.refs_1_, bf16[3,2,4096]{2,1,0:T(2,128)(2,1)S(1)} %get-tuple-element.14.refs_2_, ...), custom_call_target="tpu_custom_call" | custom-call | tf_op jit(solution)/shard_map/flush/pallas_call | solution.py:538

commit v7 on v6

--- a/solution.py
+++ b/solution.py
@@ -21,7 +21,7 @@
 OWN_FIRST = (3, -3, 1, -1)
 RELAYS_FIRST = ((3, (3, 1, -1)), (-3, (-3, 1, -1)), (6, (2, 1, -1)), (-6, (1, -1)))
 GREET = (1, -1, 2, -2, 3, -3)
-GROUPS = ((3, -3), (6, -6, 1, -1), (2, -2, 4, -4, 5, -5), (7, -7, 8))
+GROUPS = ((1, -1), (3, -3), (6, -6, 2, -2, 4, -4), (5, -5, 7, -7), (8,))
 
 
 def turned(d, side):
@@ -252,10 +252,8 @@
         (state_h, state), (wo_h, wo), (wg_h.at[0], wg), (wu_h.at[0], wu), (wd_h.at[0], wd),
     )
     pulls = [pltpu.make_async_copy(a, b, wload.at[i]) for i, (a, b) in enumerate(pairs)]
-    for p in pulls:
-        p.start()
-    early, pulls = pulls[:13], pulls[13:]
-    early[0].wait()
+    pulls[0].start()
+    pulls[0].wait()
 
     rows = tok[...].astype(F32)
     for r in range(2):
@@ -263,6 +261,9 @@
     buf[me] = tall(tokf[...], 2).astype(BF16)
     ready()
     comm.gather_start(buf, send1, recv1, OWN_FIRST)
+    for p in pulls[1:]:
+        p.start()
+    early, pulls = pulls[:13], pulls[13:]
     for p in early[1:]:
         p.wait()
     for conv, taps, dst, n in ((conv_x, conv_x_w, convx, 32), (conv_bc, conv_bc_w, convbc, 8)):
@@ -456,22 +457,16 @@
         return y * weight
 
     swaps = []
-    for ch in range(2):
-        for k in range(2):
-            half_out[ch, :, k * 512 : (k + 1) * 512] = expert(1 - core, 2 * ch + k).astype(BF16)
-        swaps.append(
-            comm.copy(half_out.at[ch], half_in.at[ch], hsend.at[ch], hrecv.at[ch], comm.partner())
-        )
-        swaps[ch].start()
-    for ch in range(2):
-        own = [expert(core, 2 * ch + k) for k in range(2)]
-        swaps[ch].wait()
-        for j in range(8):
-            k, cols = j // 4, slice(j % 4 * LANES, (j % 4 + 1) * LANES)
-            total[pl.ds(8 * ch + j, 64, stride=24), :] = own[k][:, cols] + half_in[
-                ch, :, j * LANES : (j + 1) * LANES
-            ].astype(F32)
-
+    for k in range(4):
+        half_out[k] = expert(1 - core, k).astype(BF16)
+        swaps.append(comm.copy(half_out.at[k], half_in.at[k], hsend.at[k], hrecv.at[k], comm.partner()))
+        swaps[k].start()
+    for k in range(4):
+        own = expert(core, k)
+        swaps[k].wait()
+        own = own + half_in[k].astype(F32)
+        for j in range(4):
+            total[pl.ds(4 * k + j, 64, stride=24), :] = own[:, j * LANES : (j + 1) * LANES]
 
     def pack(t, carry):
         for r in range(2):
@@ -523,11 +518,11 @@
             v((96, LANES), F32), v((24, LANES), F32),
             v((256, LANES), F32), v((256, LANES), F32), v((LANES, LANES), F32), v((32, LANES), F32),
             v((64, LANES), F32), v((64, LANES), F32), v((2, 4096), F32), v((2, 1024), F32), v((64, LANES), F32),
-            v((64, 512), BF16), v((64, LANES), F32), v((2, 64, 1024), BF16), v((2, 64, 1024), BF16),
+            v((64, 512), BF16), v((64, LANES), F32), v((4, 64, 512), BF16), v((4, 64, 512), BF16),
             v((64 * 24, LANES), F32),
             v((ep, 2, 16, LANES), BF16), v((18, 2, 16, LANES), BF16), v((8, 2, 16, LANES), BF16),
             v((14, 2, 16, LANES), BF16), v((2, 2, 16, LANES), F32),
-            dma((22,)), dma, dma((ep,)), dma, dma((ep,)), dma, dma((ep,)), dma((2,)), dma((2,)), dma, dma((ep,)),
+            dma((22,)), dma, dma((ep,)), dma, dma((ep,)), dma, dma((ep,)), dma((4,)), dma((4,)), dma, dma((ep,)),
             dma, dma((18,)), dma((14,)),
         ],
         compiler_params=pltpu.CompilerParams(

time: 75.5 us -> 75 us (level)
  no operation moved by 1% of the time
where the time goes in v7:
time: 75 us; the launch traced here: 74.8 us
  Pallas kernels  74.2 us (99%)
    pallas_call x1, Pallas kernels, layer(): pl.pallas_call(functools.partial(layer_kernel, ep, len(args), len(outs)),...  72.1 us
    pallas_call x1, Pallas kernels, layer(): pl.pallas_call(flush_kernel, out_shape=outs, in_specs=[vmem()] * len(outs...  2.06 us

profile of v7, /device:TPU:69, one launch (start us, length us, event | category | flops | bytes accessed | tf_op | source)
XLA Modules:
  0.0 74.8 jit_solution(6923727082493723097)
XLA Ops:
  0.6 72.1 %layer.1 = (bf16[2,4096]{1,0:T(2,128)(2,1)S(1)}, f32[2,64,64,128]{3,2,1,0:T(8,128)S(1)}, bf16[3,2,4096]{2,1,0:T(2,128)(2,1)S(1)}, bf16[3,2,1024]{2,1,0:T(2,128)(2,1)S(1)}) custom-call(bf16[2,4096]{1,0:T(2,128)(2,1)} %refs_0_.1, f32[32,128]{1,0:T(8,128)} %bitcast.15, bf16[4096,128]{1,0:T(8,128)(2,1)} %refs_2_.1, bf16[4096,128]{1,0:T(8,128)(2,1)} %refs_3_.1, ...), custom_call_target="tpu_custom_call" | custom-call | tf_op jit(solution)/shard_map/layer/pallas_call | solution.py:508
  72.8 2.1 %flush.1 = (bf16[2,4096]{1,0:T(2,128)(2,1)}, f32[2,64,64,128]{3,2,1,0:T(8,128)}, bf16[3,2,4096]{2,1,0:T(2,128)(2,1)}, bf16[3,2,1024]{2,1,0:T(2,128)(2,1)}) custom-call(bf16[2,4096]{1,0:T(2,128)(2,1)S(1)} %get-tuple-element.12.refs_0_, f32[2,64,64,128]{3,2,1,0:T(8,128)S(1)} %get-tuple-element.13.refs_1_, bf16[3,2,4096]{2,1,0:T(2,128)(2,1)S(1)} %get-tuple-element.14.refs_2_, ...), custom_call_target="tpu_custom_call" | custom-call | tf_op jit(solution)/shard_map/flush/pallas_call | solution.py:533
